TPU v7x, 256 devices: a whole 4x4x8 slice. The times are simulated.
256 devices in a mesh: sp: 64 (over z, y, core), tp: 4 (over x).
Axes of the slice: x: 4, y: 4, z: 8, core: 2. Of those that a mesh axis runs over, the one named last changes fastest.
Arguments:
- tokens: bfloat16 [4, 24576, 2048], P(None, 'sp'), may hold values from -21 to 21
- query_weight: bfloat16 [2048, 1024], P(None, 'tp'), may hold values from -0.125 to 0.125
- key_weight: bfloat16 [2048, 1024], P(None, 'tp'), may hold values from -0.125 to 0.125
- value_weight: bfloat16 [2048, 1024], P(None, 'tp'), may hold values from -0.125 to 0.125
- out_gain: float32 [1024], replicated, may hold values from 0.1 to 1.9
- out_weight: bfloat16 [1024, 2048], P(None, 'tp'), may hold values from -0.1875 to 0.1875
Outputs:
- mixed_out: bfloat16 [4, 24576, 2048], P(None, 'sp', 'tp')
- total_log: float32 [4, 8, 24576], P(None, 'tp', 'sp')
All inputs are finite; a program needn't handle non-finite values.
Results may differ from a plain program's by a relative error of at most 0.0098.
Values may be sent and summed in bfloat16 or wider, within the bound.
No kernel may reach another device: no remote copies, remote signals or barrier semaphores. Data moves between devices by JAX's collectives and lax.ppermute only.
A program may use at most 128 MiB of HBM per device.

v0:
```python
import math

import jax
import jax.numpy as jnp
from jax import lax
from jax.experimental import pallas as pl
from jax.experimental.pallas import tpu as pltpu
from jax.sharding import PartitionSpec as P

HEAD_DIM = 128
REACH = 64
ROPE_BASE = 10000.0
MASK_FILL = -1e30
NORM_FLOOR = 1e-06

CLASSES = 8
FAR = 16
NEAR = 4
SCALE = HEAD_DIM**-0.5
EXP2_SCALE = SCALE * math.log2(math.e)

CHUNKS = (2, 2)


def shifted(block, axis, distance):
    devices = range(lax.axis_size(axis))
    return lax.ppermute(block, axis, [(i - distance, i) for i in devices if i - distance in devices])


def turned(block, axis, distance):
    size = lax.axis_size(axis)
    return lax.ppermute(block, axis, [(i, (i + distance) % size) for i in range(size)])


def swapped(block, axis):
    return lax.ppermute(block, axis, [(i, i ^ 1) for i in range(lax.axis_size(axis))])


def row_order(length, dtype):
    dims = (CLASSES, length // CLASSES, length)
    wanted = lax.broadcasted_iota(jnp.int32, dims, 1) * CLASSES + lax.broadcasted_iota(jnp.int32, dims, 0)
    hit = lax.broadcasted_iota(jnp.int32, dims, 2) == wanted
    return jnp.where(hit, 1.0, 0.0).reshape(length, length).astype(dtype)


def rotated(projected, cosine, sine):
    heads = []
    for start in range(0, projected.shape[1], HEAD_DIM):
        head = projected[:, start : start + HEAD_DIM]
        heads.append(head * cosine + pltpu.roll(head, HEAD_DIM // 2, 1) * sine)
    return jnp.concatenate(heads, axis=1)


def project_body(turns, tokens_ref, cos_ref, sin_ref, *refs):
    weights, out_ref, order_ref = refs[: len(turns)], refs[-2], refs[-1]
    length = tokens_ref.shape[1]

    @pl.when(pl.program_id(0) == 0)
    def _():
        order_ref[...] = row_order(length, jnp.bfloat16)

    rows = tokens_ref[0]
    at = 0
    for turn, weight in zip(turns, weights):
        made = jnp.dot(rows, weight[...], preferred_element_type=jnp.float32)
        if turn:
            made = rotated(made, cos_ref[...], sin_ref[...])
        width = made.shape[1]
        moved = jnp.dot(order_ref[...], made.astype(jnp.bfloat16), preferred_element_type=jnp.float32)
        moved = moved.astype(jnp.bfloat16).reshape(CLASSES, length // CLASSES, width)
        out_ref[0, :, :, at : at + width] = moved
        at += width


def project(tokens, first, count, cosine, sine, weights, turns):
    _, length, model_dim = tokens.shape
    width = sum(w.shape[1] for w in weights)
    whole = lambda a: pl.BlockSpec(a.shape, lambda s: (0,) * a.ndim)
    return pl.pallas_call(
        lambda *refs: project_body(turns, *refs),
        grid=(count,),
        in_specs=[
            pl.BlockSpec((1, length, model_dim), lambda s: (s + first, 0, 0)),
            whole(cosine),
            whole(sine),
            *[whole(w) for w in weights],
        ],
        out_specs=pl.BlockSpec((1, CLASSES, length // CLASSES, width), lambda s: (s, 0, 0, 0)),
        out_shape=jax.ShapeDtypeStruct((count, CLASSES, length // CLASSES, width), jnp.bfloat16),
        scratch_shapes=[pltpu.VMEM((length, length), jnp.bfloat16)],
        cost_estimate=pl.CostEstimate(
            flops=2 * count * length * model_dim * width,
            transcendentals=0,
            bytes_accessed=2 * (count * length * (model_dim + width) + model_dim * width),
        ),
    )(tokens, cosine, sine, *weights)


def attend_body(
    blocks, place_ref, q_ref, own_ref, first_ref, second_ref, left2_ref, right2_ref, left3_ref, right3_ref,
    out_ref, log_ref, left1, right1, far_bias, near_bias, unit_bias, acc, peak, total, logs, order
):
    per = q_ref.shape[2]
    channels = q_ref.shape[3]
    heads = channels // HEAD_DIM
    reach_far = REACH * FAR // CLASSES
    reach_near = REACH * NEAR // CLASSES
    tile = 16
    start = place_ref[0] * per
    limit = blocks * per
    south = place_ref[1]

    @pl.when(pl.program_id(0) == 0)
    def _():
        order[...] = row_order(CLASSES * per, jnp.bfloat16)

        def filled(ok, row):
            return jnp.where(ok & (row >= 0) & (row < limit), 0.0, MASK_FILL)

        dims = far_bias.shape
        query = lax.broadcasted_iota(jnp.int32, dims, 0)
        key = lax.broadcasted_iota(jnp.int32, dims, 1) - reach_far
        step = key - query
        far_bias[...] = filled((jnp.abs(step) <= reach_far) & ((step & 1) == 0), start + key)
        span = per + 2 * reach_near
        dims = (2, per, 2, span)
        for a in range(2):
            for b in range(2):
                dims = (per, span)
                query = lax.broadcasted_iota(jnp.int32, dims, 0)
                key = lax.broadcasted_iota(jnp.int32, dims, 1) - reach_near
                step = 2 * (key - query) + (b - a)
                near_bias[a * per : (a + 1) * per, b * span : (b + 1) * span] = filled(
                    jnp.abs(step) <= REACH, start + key
                )
        wide = 3 * tile
        dims = (CLASSES, tile, CLASSES * wide)
        query = lax.broadcasted_iota(jnp.int32, dims, 1) * CLASSES + lax.broadcasted_iota(jnp.int32, dims, 0)
        lane = lax.broadcasted_iota(jnp.int32, dims, 2)
        kind = lane // wide
        row = lane - kind * wide - tile
        near = jnp.abs(row * CLASSES + kind - query) <= REACH
        for t in range(per // tile):
            unit_bias[t] = filled(near, start + tile * t + row).reshape(CLASSES * tile, CLASSES * wide)

    left1[...] = jnp.where(south == 1, second_ref[0], first_ref[0])
    right1[...] = jnp.where(south == 1, first_ref[0], second_ref[0])

    def soft(q, k, v, bias):
        scores = lax.dot_general(q, k, (((1,), (1,)), ((), ())), preferred_element_type=jnp.float32) + bias
        top = jnp.max(scores, axis=1, keepdims=True)
        weights = jnp.exp2((scores - top) * EXP2_SCALE)
        weight_sum = jnp.sum(weights, axis=1, keepdims=True)
        summed = jnp.dot(weights.astype(jnp.bfloat16), v, preferred_element_type=jnp.float32)
        return top, weight_sum, summed

    for h in range(heads):
        ql = slice(h * HEAD_DIM, (h + 1) * HEAD_DIM)
        kl = ql
        vl = slice(channels + h * HEAD_DIM, channels + (h + 1) * HEAD_DIM)
        blocks_of = per // tile
        for t in range(blocks_of):
            here = slice(t * tile, (t + 1) * tile)
            lo, hi = tile * (t - 1), tile * (t + 2)

            def around(lanes):
                parts = []
                if lo < 0:
                    parts.append(left1[:, per + lo : per, lanes])
                parts.append(own_ref[0, :, max(lo, 0) : min(hi, per), lanes])
                if hi > per:
                    parts.append(right1[:, 0 : hi - per, lanes])
                joined = jnp.concatenate(parts, axis=1) if len(parts) > 1 else parts[0]
                return joined.reshape(CLASSES * 3 * tile, HEAD_DIM)

            q = q_ref[0, :, here, ql].reshape(CLASSES * tile, HEAD_DIM)
            top, weight_sum, summed = soft(q, around(kl), around(vl), unit_bias[t])
            dims = (CLASSES, tile, HEAD_DIM)
            acc[:, here, :] = summed.reshape(dims)
            peak[:, here, :] = jnp.broadcast_to(top, (CLASSES * tile, HEAD_DIM)).reshape(dims)
            total[:, here, :] = jnp.broadcast_to(weight_sum, (CLASSES * tile, HEAD_DIM)).reshape(dims)
        half = CLASSES // 2
        for c in range(half):

            def around(lanes):
                parts = []
                for r in (c, c + half):
                    parts += [left1[r, per - reach_near : per, lanes], own_ref[0, r, :, lanes], right1[r, 0:reach_near, lanes]]
                return jnp.concatenate(parts, axis=0)

            q = jnp.concatenate([q_ref[0, c, :, ql], q_ref[0, c + half, :, ql]], axis=0)
            top, weight_sum, summed = soft(q, around(kl), around(vl), near_bias[...])
            for n, r in enumerate((c, c + half)):
                rows = slice(n * per, (n + 1) * per)
                old = peak[r]
                new = jnp.maximum(old, top[rows])
                keep = jnp.exp2((old - new) * EXP2_SCALE)
                add = jnp.exp2((top[rows] - new) * EXP2_SCALE)
                acc[r] = acc[r] * keep + summed[rows] * add
                total[r] = total[r] * keep + weight_sum[rows] * add
                peak[r] = new
        for r in range(CLASSES):

            def around(lanes):
                return jnp.concatenate(
                    [
                        left3_ref[0, r, :, lanes],
                        left2_ref[0, r, :, lanes],
                        left1[r, :, lanes],
                        own_ref[0, r, :, lanes],
                        right1[r, :, lanes],
                        right2_ref[0, r, :, lanes],
                        right3_ref[0, r, :, lanes],
                    ],
                    axis=0,
                )

            top, weight_sum, summed = soft(q_ref[0, r, :, ql], around(kl), around(vl), far_bias[...])
            old = peak[r]
            new = jnp.maximum(old, top)
            keep = jnp.exp2((old - new) * EXP2_SCALE)
            add = jnp.exp2((top - new) * EXP2_SCALE)
            whole = total[r] * keep + weight_sum * add
            out_ref[0, r * per : (r + 1) * per, ql] = ((acc[r] * keep + summed * add) / whole).astype(jnp.bfloat16)
            log = new * SCALE + jnp.log(whole)
            rows = slice(r * per, (r + 1) * per)
            if h == 0:
                logs[rows] = log
            else:
                lane = lax.broadcasted_iota(jnp.int32, (per, HEAD_DIM), 1)
                logs[rows] = jnp.where(lane == h, log, logs[rows])
    left = logs[...]
    natural = jnp.zeros((HEAD_DIM, CLASSES * per), jnp.float32)
    for _ in range(3):
        part = left.astype(jnp.bfloat16)
        natural += lax.dot_general(part, order[...], (((0,), (0,)), ((), ())), preferred_element_type=jnp.float32)
        left = left - part.astype(jnp.float32)
    log_ref[0] = natural[0:heads]


def attend(place, blocks, q, first, own, swap_own, swap_far, left2, right2, left3, right3):
    count, classes, per, both = own.shape
    channels = both // 2
    heads = channels // HEAD_DIM
    length = classes * per
    edge = left3.shape[2]
    reach_near = REACH * NEAR // CLASSES
    whole = pl.BlockSpec((1, classes, per, both), lambda s, p: (s, 0, 0, 0))
    part = pl.BlockSpec((1, classes, edge, both), lambda s, p: (s, 0, 0, 0))
    f32 = jnp.float32
    far_keys = per + 2 * REACH * FAR // CLASSES
    near_keys = 2 * (per + 2 * reach_near)
    return pl.pallas_call(
        lambda *refs: attend_body(blocks, *refs),
        grid_spec=pltpu.PrefetchScalarGridSpec(
            num_scalar_prefetch=1,
            grid=(count,),
            in_specs=[
                pl.BlockSpec((1, classes, per, channels), lambda s, p: (s + first, 0, 0, 0)),
                whole, whole, whole, whole, whole, part, part,
            ],
            out_specs=[
                pl.BlockSpec((1, length, channels), lambda s, p: (s, 0, 0)),
                pl.BlockSpec((1, heads, length), lambda s, p: (s, 0, 0)),
            ],
            scratch_shapes=[
                pltpu.VMEM((classes, per, both), jnp.bfloat16),
                pltpu.VMEM((classes, per, both), jnp.bfloat16),
                pltpu.VMEM((per, far_keys), f32),
                pltpu.VMEM((2 * per, near_keys), f32),
                pltpu.VMEM((per // 16, classes * 16, classes * 48), f32),
                pltpu.VMEM((classes, per, HEAD_DIM), f32),
                pltpu.VMEM((classes, per, HEAD_DIM), f32),
                pltpu.VMEM((classes, per, HEAD_DIM), f32),
                pltpu.VMEM((length, HEAD_DIM), f32),
                pltpu.VMEM((length, length), jnp.bfloat16),
            ],
        ),
        out_shape=[
            jax.ShapeDtypeStruct((count, length, channels), jnp.bfloat16),
            jax.ShapeDtypeStruct((count, heads, length), f32),
        ],
        cost_estimate=pl.CostEstimate(
            flops=4 * count * length * channels * (far_keys + near_keys + 3 * classes * 48) * 4,
            transcendentals=count * heads * length * 800,
            bytes_accessed=2 * count * length * both * 6,
        ),
    )(place, q, own, swap_own, swap_far, left2, right2, left3, right3)


def finish_body(channels_all, place_ref, *refs):
    parts, gains, weights = refs[0:5], refs[5:9], refs[9:13]
    out_ref, order = refs[13], refs[14]
    own, before, after, low, high = parts
    length = own.shape[1]

    @pl.when(pl.program_id(0) == 0)
    def _():
        order[...] = row_order(length, jnp.bfloat16)

    opposite = jnp.concatenate([low[0], high[0]], axis=0)
    projected = None
    square = None
    for value, gain, weight in zip((own[0], before[0], after[0], opposite), gains, weights):
        lifted = value.astype(jnp.float32)
        scaled = (lifted * gain[...]).astype(jnp.bfloat16)
        term = jnp.dot(scaled, weight[...], preferred_element_type=jnp.float32)
        squares = jnp.sum(lifted * lifted, axis=1, keepdims=True)
        projected = term if projected is None else projected + term
        square = squares if square is None else square + squares
    mixed = (projected * lax.rsqrt(square / channels_all + NORM_FLOOR)).astype(jnp.bfloat16)
    natural = lax.dot_general(order[...], mixed, (((0,), (0,)), ((), ())), preferred_element_type=jnp.float32)
    out_ref[0] = natural.astype(jnp.bfloat16)


def finish(place, merged, before, after, low, high, gain, weight, ranks):
    count, length, channels = merged.shape
    half = length // 2
    channels_all, width = weight.shape
    block = pl.BlockSpec((1, length, channels), lambda s, p: (s, 0, 0))
    part = pl.BlockSpec((1, half, channels), lambda s, p: (s, 0, 0))
    turns = (0, ranks - 1, 1, 2)

    def gain_at(turn):
        return pl.BlockSpec((1, channels), lambda s, p: (0, lax.rem(p[2] + turn, ranks)))

    def weight_at(turn):
        return pl.BlockSpec((channels, width), lambda s, p: (lax.rem(p[2] + turn, ranks), 0))

    return pl.pallas_call(
        lambda *refs: finish_body(channels_all, *refs),
        grid_spec=pltpu.PrefetchScalarGridSpec(
            num_scalar_prefetch=1,
            grid=(count,),
            in_specs=[block, block, block, part, part, *map(gain_at, turns), *map(weight_at, turns)],
            out_specs=pl.BlockSpec((1, length, width), lambda s, p: (s, 0, 0)),
            scratch_shapes=[pltpu.VMEM((length, length), jnp.bfloat16)],
        ),
        out_shape=jax.ShapeDtypeStruct((count, length, width), jnp.bfloat16),
        cost_estimate=pl.CostEstimate(
            flops=2 * count * length * channels_all * width,
            transcendentals=0,
            bytes_accessed=2 * (count * length * (channels_all + width) + channels_all * width),
        ),
    )(place, merged, before, after, low, high, *[gain] * 4, *[weight] * 4)


def shards(tokens, query_weight, key_weight, value_weight, out_gain, out_weight):
    seq_count, length, model_dim = tokens.shape
    at = lax.axis_index("sp")
    core = at % 2
    rank = lax.axis_index("tp")
    ranks = lax.axis_size("tp")
    blocks = lax.axis_size("sp")
    place = jnp.stack([at, 1 - core, rank]).astype(jnp.int32)
    positions = at * length + jnp.arange(length, dtype=jnp.int32)
    half_dim = HEAD_DIM // 2
    frequency = ROPE_BASE ** (-jnp.arange(half_dim, dtype=jnp.float32) / half_dim)
    angles = positions.astype(jnp.float32)[:, None] * frequency[None, :]
    cosine = jnp.cos(angles)
    sine = jnp.sin(angles)
    cosine = jnp.concatenate([cosine, cosine], axis=1)
    sine = jnp.concatenate([-sine, sine], axis=1)
    per = length // CLASSES
    edge = REACH * FAR // CLASSES - 2 * per

    gain = out_gain.reshape(1, -1)
    mixed_all, logs_all = [], []
    first = 0
    stage = []
    for count in CHUNKS:
        own = project(tokens, first, count, cosine, sine, (key_weight, value_weight), (True, False))
        left2 = shifted(own, "sp", 2)
        right2 = shifted(own, "sp", -2)
        swap_own = swapped(own, "sp")
        stage.append((first, count, own, left2, right2, swap_own))
        first += count
    queries = project(tokens, 0, seq_count, cosine, sine, (query_weight,), (True,))
    for first, count, own, left2, right2, swap_own in stage:
        swap_far = swapped(jnp.where(core == 1, left2, right2), "sp")
        left3 = shifted(left2[:, :, per - edge :], "sp", 1)
        right3 = shifted(right2[:, :, :edge], "sp", -1)
        merged, logs = attend(
            place, blocks, queries, first, own, swap_own, swap_far, left2, right2, left3, right3
        )
        before = turned(merged, "tp", 1)
        after = turned(merged, "tp", -1)
        low = turned(before[:, : length // 2], "tp", 1)
        high = turned(after[:, length // 2 :], "tp", -1)
        mixed_all.append(finish(place, merged, before, after, low, high, gain, out_weight, ranks))
        logs_all.append(logs)
    return (jnp.concatenate(mixed_all, axis=0), jnp.concatenate(logs_all, axis=0))


def solution(mesh):
    return jax.shard_map(
        shards,
        mesh=mesh,
        in_specs=(
            P(None, "sp", None),
            P(None, "tp"),
            P(None, "tp"),
            P(None, "tp"),
            P(),
            P(None, "tp"),
        ),
        out_specs=(P(None, "sp", "tp"), P(None, "tp", "sp")),
        check_vma=False,
    )
```

profile of v0, /device:TPU:128, one launch (start us, length us, event | category | flops | bytes accessed | tf_op | source)
XLA Modules:
  0.0 146.7 jit_solution(13664502876192678589)
XLA Ops:
  0.7 0.8 fusion
  1.4 0.9 pad_maximum_fusion.1
  2.4 7.8 %shard_map.78.refs_2_ = bf16[2,8,48,512]{3,2,1,0:T(8,128)(2,1)} custom-call(bf16[4,384,2048]{2,1,0:T(8,128)(2,1)} %refs_0_.5, f32[384,128]{1,0:T(8,128)} %get-tuple-element.13.refs_1_, f32[384,128]{1,0:T(8,128)} %get-tuple-element.14.refs_2_, bf16[2048,256]{1,0:T(8,128)(2,1)} %refs_3_.5, bf16[2048,256]{1,0:T(8,128)(2,1)} %refs_4_.3), custom_call_target="tpu_custom_call" | custom-call | flops 1610612736 | bytes 6029312 | tf_op jit(solution)/shard_map/pallas_call | solution.py:79
  10.2 3.5 %collective-permute-start.1 = (bf16[2,8,48,512]{3,2,1,0:T(8,128)(2,1)}, bf16[2,8,48,512]{3,2,1,0:T(8,128)(2,1)S(1)}, u32[]{:S(2)}, u32[]{:S(2)}) collective-permute-start(bf16[2,8,48,512]{3,2,1,0:T(8,128)(2,1)} %shard_map.78.refs_2_), channel_id=1, source_target_pairs={{0,8},{4,12},{8,16},{12,20},{16,24},{20,28},{24,32},{28,36},{32,40... | collective-permute-start | bytes 2359304 | tf_op jit(solution)/shard_map/ppermute | solution.py:27
  13.7 5.7 %collective-permute-start.2 = (bf16[2,8,48,512]{3,2,1,0:T(8,128)(2,1)}, bf16[2,8,48,512]{3,2,1,0:T(8,128)(2,1)S(1)}, u32[]{:S(2)}, u32[]{:S(2)}) collective-permute-start(bf16[2,8,48,512]{3,2,1,0:T(8,128)(2,1)} %shard_map.78.refs_2_), channel_id=1, source_target_pairs={{8,0},{12,4},{16,8},{20,12},{24,16},{28,20},{32,24},{36,28},{40,32... | collective-permute-start | bytes 2359304 | tf_op jit(solution)/shard_map/ppermute | solution.py:27
  19.3 7.8 %shard_map.81.refs_2_ = bf16[2,8,48,512]{3,2,1,0:T(8,128)(2,1)} custom-call(bf16[4,384,2048]{2,1,0:T(8,128)(2,1)} %refs_0_.5, f32[384,128]{1,0:T(8,128)} %get-tuple-element.13.refs_1_, f32[384,128]{1,0:T(8,128)} %get-tuple-element.14.refs_2_, bf16[2048,256]{1,0:T(8,128)(2,1)} %refs_3_.5, bf16[2048,256]{1,0:T(8,128)(2,1)} %refs_4_.3), custom_call_target="tpu_custom_call" | custom-call | flops 1610612736 | bytes 6029312 | tf_op jit(solution)/shard_map/pallas_call | solution.py:79
  27.2 1.9 %collective-permute-start.11 = (bf16[2,8,48,512]{3,2,1,0:T(8,128)(2,1)}, bf16[2,8,48,512]{3,2,1,0:T(8,128)(2,1)S(1)}, u32[]{:S(2)}, u32[]{:S(2)}) collective-permute-start(bf16[2,8,48,512]{3,2,1,0:T(8,128)(2,1)} %shard_map.81.refs_2_), channel_id=1, source_target_pairs={{0,8},{4,12},{8,16},{12,20},{16,24},{20,28},{24,32},{28,36},{32,40... | collective-permute-start | bytes 2359304 | tf_op jit(solution)/shard_map/ppermute | solution.py:27
  29.1 7.2 %collective-permute-start.12 = (bf16[2,8,48,512]{3,2,1,0:T(8,128)(2,1)}, bf16[2,8,48,512]{3,2,1,0:T(8,128)(2,1)S(1)}, u32[]{:S(2)}, u32[]{:S(2)}) collective-permute-start(bf16[2,8,48,512]{3,2,1,0:T(8,128)(2,1)} %shard_map.81.refs_2_), channel_id=1, source_target_pairs={{8,0},{12,4},{16,8},{20,12},{24,16},{28,20},{32,24},{36,28},{40,32... | collective-permute-start | bytes 2359304 | tf_op jit(solution)/shard_map/ppermute | solution.py:27
  36.3 0.1 collective-permute-start
  36.4 0.0 collective-permute-done.1.refs_5_
  36.5 0.1 collective-permute-done.2.refs_6_
  36.6 1.2 broadcast_select_fusion.1
  37.7 0.3 collective-permute-start.3
  38.0 0.9 slice.32
  38.9 0.0 copy-done.3
  38.9 2.1 %collective-permute-start.4 = (bf16[2,8,32,512]{3,2,1,0:T(8,128)(2,1)}, bf16[2,8,32,512]{3,2,1,0:T(8,128)(2,1)}, u32[]{:S(2)}, u32[]{:S(2)}) collective-permute-start(bf16[2,8,32,512]{3,2,1,0:T(8,128)(2,1)} %slice.32), channel_id=1, source_target_pairs={{0,4},{4,8},{8,12},{12,16},{16,20},{20,24},{24,28},{28,32},{32,36}... | collective-permute-start | bytes 1572872 | tf_op jit(solution)/shard_map/ppermute | solution.py:27
  41.0 0.8 slice.33
  41.9 11.1 %collective-permute-done.11.refs_5_ = bf16[2,8,48,512]{3,2,1,0:T(8,128)(2,1)S(1)} collective-permute-done((bf16[2,8,48,512]{3,2,1,0:T(8,128)(2,1)}, bf16[2,8,48,512]{3,2,1,0:T(8,128)(2,1)S(1)}, u32[]{:S(2)}, u32[]{:S(2)}) %collective-permute-start.11) | collective-permute-done | bytes 786464 | tf_op jit(solution)/shard_map/ppermute | solution.py:27
  53.0 1.9 %collective-permute-start.5 = (bf16[2,8,32,512]{3,2,1,0:T(8,128)(2,1)}, bf16[2,8,32,512]{3,2,1,0:T(8,128)(2,1)}, u32[]{:S(2)}, u32[]{:S(2)}) collective-permute-start(bf16[2,8,32,512]{3,2,1,0:T(8,128)(2,1)} %slice.33), channel_id=1, source_target_pairs={{4,0},{8,4},{12,8},{16,12},{20,16},{24,20},{28,24},{32,28},{36,32}... | collective-permute-start | bytes 1572872 | tf_op jit(solution)/shard_map/ppermute | solution.py:27
  54.9 0.0 collective-permute-done.12.refs_6_
  54.9 0.6 collective-permute-start.10
  55.5 0.1 broadcast_select_fusion
  55.6 0.0 collective-permute-done.refs_3_
  55.6 0.1 collective-permute-start.13
  55.7 7.3 %shard_map.77.refs_1_ = bf16[4,8,48,256]{3,2,1,0:T(8,128)(2,1)} custom-call(bf16[4,384,2048]{2,1,0:T(8,128)(2,1)} %refs_0_.5, f32[384,128]{1,0:T(8,128)} %get-tuple-element.13.refs_1_, f32[384,128]{1,0:T(8,128)} %get-tuple-element.14.refs_2_, bf16[2048,256]{1,0:T(8,128)(2,1)} %refs_3_.3), custom_call_target="tpu_custom_call" | custom-call | flops 1610612736 | bytes 8126464 | tf_op jit(solution)/shard_map/pallas_call | solution.py:79
  63.1 0.0 collective-permute-done.4.refs_7_
  63.1 2.4 %collective-permute-start.14 = (bf16[2,8,32,512]{3,2,1,0:T(8,128)(2,1)S(1)}, bf16[2,8,32,512]{3,2,1,0:T(8,128)(2,1)S(1)}, u32[]{:S(2)}, u32[]{:S(2)}) collective-permute-start(bf16[2,8,32,512]{3,2,1,0:T(8,128)(2,1)S(1)} %slice.36), channel_id=1, source_target_pairs={{0,4},{4,8},{8,12},{12,16},{16,20},{20,24},{24,28},{28,32},{32,36}... | collective-permute-start | bytes 1572872 | tf_op jit(solution)/shard_map/ppermute | solution.py:27
  65.5 0.0 collective-permute-done.5.refs_8_
  65.5 6.7 %collective-permute-start.15 = (bf16[2,8,32,512]{3,2,1,0:T(8,128)(2,1)S(1)}, bf16[2,8,32,512]{3,2,1,0:T(8,128)(2,1)}, u32[]{:S(2)}, u32[]{:S(2)}) collective-permute-start(bf16[2,8,32,512]{3,2,1,0:T(8,128)(2,1)S(1)} %slice.37), channel_id=1, source_target_pairs={{4,0},{8,4},{12,8},{16,12},{20,16},{24,20},{28,24},{32,28},{36,32}... | collective-permute-start | bytes 1572872 | tf_op jit(solution)/shard_map/ppermute | solution.py:27
  72.2 0.6 pad_add_fusion.refs_0_
  72.8 0.0 collective-permute-done.3.refs_4_
  72.8 19.5 %shard_map.79 = (bf16[2,384,256]{2,1,0:T(8,128)(2,1)}, f32[2,2,384]{2,1,0:T(2,128)}) custom-call(s32[3]{0:T(128)} %pad_add_fusion.refs_0_, bf16[4,8,48,256]{3,2,1,0:T(8,128)(2,1)} %shard_map.77.refs_1_, bf16[2,8,48,512]{3,2,1,0:T(8,128)(2,1)} %shard_map.78.refs_2_, bf16[2,8,48,512]{3,2,1,0:T(8,128)(2,1)} %collective-permute-done.refs_3_, ...), custom_call_target="tpu_custom_call" | custom-call | flops 5284823040 | bytes 4718592 | tf_op jit(solution)/shard_map/pallas_call | solution.py:253
  92.3 1.5 %collective-permute-start.6 = (bf16[2,384,256]{2,1,0:T(8,128)(2,1)}, bf16[2,384,256]{2,1,0:T(8,128)(2,1)S(1)}, u32[]{:S(2)}, u32[]{:S(2)}) collective-permute-start(bf16[2,384,256]{2,1,0:T(8,128)(2,1)} %get-tuple-element.6.refs_1_), channel_id=1, source_target_pairs={{0,1},{1,2},{2,3},{3,0},{4,5},{5,6},{6,7},{7,4},{8,9},{9,10},{10,1... | collective-permute-start | bytes 1179656 | tf_op jit(solution)/shard_map/ppermute | solution.py:32
  93.8 0.0 collective-permute-done.10.refs_3_
  93.8 1.7 %collective-permute-start.7 = (bf16[2,384,256]{2,1,0:T(8,128)(2,1)}, bf16[2,384,256]{2,1,0:T(8,128)(2,1)S(1)}, u32[]{:S(2)}, u32[]{:S(2)}) collective-permute-start(bf16[2,384,256]{2,1,0:T(8,128)(2,1)} %get-tuple-element.6.refs_1_), channel_id=1, source_target_pairs={{0,3},{1,0},{2,1},{3,2},{4,7},{5,4},{6,5},{7,6},{8,11},{9,8},{10,9... | collective-permute-start | bytes 1179656 | tf_op jit(solution)/shard_map/ppermute | solution.py:32
  95.5 0.0 collective-permute-done.14.refs_7_
  95.5 0.0 collective-permute-done.15.refs_8_
  95.5 0.0 collective-permute-done.13.refs_4_
  95.6 0.8 copy-done.15
  96.3 19.5 %shard_map.82 = (bf16[2,384,256]{2,1,0:T(8,128)(2,1)}, f32[2,2,384]{2,1,0:T(2,128)}) custom-call(s32[3]{0:T(128)} %pad_add_fusion.refs_0_, bf16[4,8,48,256]{3,2,1,0:T(8,128)(2,1)} %shard_map.77.refs_1_, bf16[2,8,48,512]{3,2,1,0:T(8,128)(2,1)} %shard_map.81.refs_2_, bf16[2,8,48,512]{3,2,1,0:T(8,128)(2,1)} %collective-permute-done.10.refs_3_, ...), custom_call_target="tpu_custom_call" | custom-call | flops 5284823040 | bytes 4718592 | tf_op jit(solution)/shard_map/pallas_call | solution.py:253
  115.8 0.0 copy-start.14
  115.8 0.4 collective-permute-start.16
  116.2 3.0 %collective-permute-start.17 = (bf16[2,384,256]{2,1,0:T(8,128)(2,1)}, bf16[2,384,256]{2,1,0:T(8,128)(2,1)S(1)}, u32[]{:S(2)}, u32[]{:S(2)}) collective-permute-start(bf16[2,384,256]{2,1,0:T(8,128)(2,1)} %get-tuple-element.7.refs_1_), channel_id=1, source_target_pairs={{0,3},{1,0},{2,1},{3,2},{4,7},{5,4},{6,5},{7,6},{8,11},{9,8},{10,9... | collective-permute-start | bytes 1179656 | tf_op jit(solution)/shard_map/ppermute | solution.py:32
  119.1 0.0 collective-permute-done.6.refs_2_
  119.2 0.3 collective-permute-start.8
  119.5 0.0 collective-permute-done.7.refs_3_
  119.5 3.3 %collective-permute-start.9 = (bf16[2,192,256]{2,1,0:T(8,128)(2,1)S(1)}, bf16[2,192,256]{2,1,0:T(8,128)(2,1)S(1)}, u32[]{:S(2)}, u32[]{:S(2)}) collective-permute-start(bf16[2,192,256]{2,1,0:T(8,128)(2,1)S(1)} %slice.35), channel_id=1, source_target_pairs={{0,3},{1,0},{2,1},{3,2},{4,7},{5,4},{6,5},{7,6},{8,11},{9,8},{10,9... | collective-permute-start | bytes 589832 | tf_op jit(solution)/shard_map/ppermute | solution.py:32
  122.8 5.1 %collective-permute-done.16.refs_2_ = bf16[2,384,256]{2,1,0:T(8,128)(2,1)S(1)} collective-permute-done((bf16[2,384,256]{2,1,0:T(8,128)(2,1)}, bf16[2,384,256]{2,1,0:T(8,128)(2,1)S(1)}, u32[]{:S(2)}, u32[]{:S(2)}) %collective-permute-start.16) | collective-permute-done | bytes 393248 | tf_op jit(solution)/shard_map/ppermute | solution.py:32
  127.9 0.1 collective-permute-start.18
  128.0 0.0 collective-permute-done.17.refs_3_
  128.1 3.3 %collective-permute-start.19 = (bf16[2,192,256]{2,1,0:T(8,128)(2,1)S(1)}, bf16[2,192,256]{2,1,0:T(8,128)(2,1)S(1)}, u32[]{:S(2)}, u32[]{:S(2)}) collective-permute-start(bf16[2,192,256]{2,1,0:T(8,128)(2,1)S(1)} %slice.39), channel_id=1, source_target_pairs={{0,3},{1,0},{2,1},{3,2},{4,7},{5,4},{6,5},{7,6},{8,11},{9,8},{10,9... | collective-permute-start | bytes 589832 | tf_op jit(solution)/shard_map/ppermute | solution.py:32
  131.4 0.6 pad_maximum_fusion.3
  132.0 0.0 collective-permute-done.8.refs_4_
  132.0 0.0 collective-permute-done.9.refs_5_
  132.0 0.6 copy-done.9
  132.6 0.1 copy-done.11
  132.7 5.1 %shard_map.80 = bf16[2,384,512]{2,1,0:T(8,128)(2,1)} custom-call(s32[3]{0:T(128)} %pad_add_fusion.refs_0_, bf16[2,384,256]{2,1,0:T(8,128)(2,1)} %get-tuple-element.6.refs_1_, bf16[2,384,256]{2,1,0:T(8,128)(2,1)} %copy-done.5, bf16[2,384,256]{2,1,0:T(8,128)(2,1)} %copy-done.6, bf16[2,192,256]{2,1,0:T(8,128)(2,1)} %copy-done.9, ...), custom_call_target="tpu_custom_call" | custom-call | flops 805306368 | bytes 3407872 | tf_op jit(solution)/shard_map/pallas_call | solution.py:330
  137.8 0.0 copy-start
  137.8 0.0 collective-permute-done.18.refs_4_
  137.8 0.0 collective-permute-done.19.refs_5_
  137.8 0.7 copy-done.10
  138.5 0.7 copy-done.12
  139.2 5.1 %shard_map.83 = bf16[2,384,512]{2,1,0:T(8,128)(2,1)} custom-call(s32[3]{0:T(128)} %pad_add_fusion.refs_0_, bf16[2,384,256]{2,1,0:T(8,128)(2,1)} %get-tuple-element.7.refs_1_, bf16[2,384,256]{2,1,0:T(8,128)(2,1)} %copy-done.7, bf16[2,384,256]{2,1,0:T(8,128)(2,1)} %copy-done.8, bf16[2,192,256]{2,1,0:T(8,128)(2,1)} %copy-done.10, ...), custom_call_target="tpu_custom_call" | custom-call | flops 805306368 | bytes 3407872 | tf_op jit(solution)/shard_map/pallas_call | solution.py:330
  144.3 2.4 %pad_maximum_fusion = bf16[4,384,512]{2,1,0:T(8,128)(2,1)} fusion(bf16[2,384,512]{2,1,0:T(8,128)(2,1)} %shard_map.83, bf16[2,384,512]{2,1,0:T(8,128)(2,1)S(1)} %copy-done), kind=kLoop, calls=%fused_computation | loop fusion | flops 786432 | bytes 3145728 | tf_op jit(solution)/shard_map/concatenate | solution.py:392
  (32 shorter events, 0.2 us)
Async XLA Ops:
  10.2 26.3 %collective-permute-start.1 = (bf16[2,8,48,512]{3,2,1,0:T(8,128)(2,1)}, bf16[2,8,48,512]{3,2,1,0:T(8,128)(2,1)S(1)}, u32[]{:S(2)}, u32[]{:S(2)}) collective-permute-start(bf16[2,8,48,512]{3,2,1,0:T(8,128)(2,1)} %shard_map.78.refs_2_), channel_id=1, source_target_pairs={{0,8},{4,12},{8,16},{12,20},{16,24},{20,28},{24,32},{28,36},{32,40... | collective-permute-start | bytes 2359304 | tf_op jit(solution)/shard_map/ppermute | solution.py:27
  13.7 22.9 %collective-permute-start.2 = (bf16[2,8,48,512]{3,2,1,0:T(8,128)(2,1)}, bf16[2,8,48,512]{3,2,1,0:T(8,128)(2,1)S(1)}, u32[]{:S(2)}, u32[]{:S(2)}) collective-permute-start(bf16[2,8,48,512]{3,2,1,0:T(8,128)(2,1)} %shard_map.78.refs_2_), channel_id=1, source_target_pairs={{8,0},{12,4},{16,8},{20,12},{24,16},{28,20},{32,24},{36,28},{40,32... | collective-permute-start | bytes 2359304 | tf_op jit(solution)/shard_map/ppermute | solution.py:27
  27.2 25.8 %collective-permute-start.11 = (bf16[2,8,48,512]{3,2,1,0:T(8,128)(2,1)}, bf16[2,8,48,512]{3,2,1,0:T(8,128)(2,1)S(1)}, u32[]{:S(2)}, u32[]{:S(2)}) collective-permute-start(bf16[2,8,48,512]{3,2,1,0:T(8,128)(2,1)} %shard_map.81.refs_2_), channel_id=1, source_target_pairs={{0,8},{4,12},{8,16},{12,20},{16,24},{20,28},{24,32},{28,36},{32,40... | collective-permute-start | bytes 2359304 | tf_op jit(solution)/shard_map/ppermute | solution.py:27
  29.1 25.8 %collective-permute-start.12 = (bf16[2,8,48,512]{3,2,1,0:T(8,128)(2,1)}, bf16[2,8,48,512]{3,2,1,0:T(8,128)(2,1)S(1)}, u32[]{:S(2)}, u32[]{:S(2)}) collective-permute-start(bf16[2,8,48,512]{3,2,1,0:T(8,128)(2,1)} %shard_map.81.refs_2_), channel_id=1, source_target_pairs={{8,0},{12,4},{16,8},{20,12},{24,16},{28,20},{32,24},{36,28},{40,32... | collective-permute-start | bytes 2359304 | tf_op jit(solution)/shard_map/ppermute | solution.py:27
  36.3 19.3 %collective-permute-start = (bf16[2,8,48,512]{3,2,1,0:T(8,128)(2,1)}, bf16[2,8,48,512]{3,2,1,0:T(8,128)(2,1)}, u32[]{:S(2)}, u32[]{:S(2)}) collective-permute-start(bf16[2,8,48,512]{3,2,1,0:T(8,128)(2,1)} %shard_map.78.refs_2_), channel_id=1, source_target_pairs={{0,4},{4,0},{8,12},{12,8},{16,20},{20,16},{24,28},{28,24},{32,36},... | collective-permute-start | bytes 2359304 | tf_op jit(solution)/shard_map/ppermute | solution.py:36
  36.4 2.5 %copy-start.3 = (bf16[2,8,48,512]{3,2,1,0:T(8,128)(2,1)}, bf16[2,8,48,512]{3,2,1,0:T(8,128)(2,1)S(1)}, u32[]{:S(2)}) copy-start(bf16[2,8,48,512]{3,2,1,0:T(8,128)(2,1)S(1)} %collective-permute-done.1.refs_5_) | copy-start | bytes 2359300
  36.6 4.5 %copy-start.4 = (bf16[2,8,48,512]{3,2,1,0:T(8,128)(2,1)}, bf16[2,8,48,512]{3,2,1,0:T(8,128)(2,1)S(1)}, u32[]{:S(2)}) copy-start(bf16[2,8,48,512]{3,2,1,0:T(8,128)(2,1)S(1)} %collective-permute-done.2.refs_6_) | copy-start | bytes 2359300
  37.7 35.1 %collective-permute-start.3 = (bf16[2,8,48,512]{3,2,1,0:T(8,128)(2,1)}, bf16[2,8,48,512]{3,2,1,0:T(8,128)(2,1)}, u32[]{:S(2)}, u32[]{:S(2)}) collective-permute-start(bf16[2,8,48,512]{3,2,1,0:T(8,128)(2,1)} %broadcast_select_fusion.1), channel_id=1, source_target_pairs={{0,4},{4,0},{8,12},{12,8},{16,20},{20,16},{24,28},{28,24},{32,36},... | collective-permute-start | bytes 2359304 | tf_op jit(solution)/shard_map/ppermute | solution.py:36
  38.9 24.2 %collective-permute-start.4 = (bf16[2,8,32,512]{3,2,1,0:T(8,128)(2,1)}, bf16[2,8,32,512]{3,2,1,0:T(8,128)(2,1)}, u32[]{:S(2)}, u32[]{:S(2)}) collective-permute-start(bf16[2,8,32,512]{3,2,1,0:T(8,128)(2,1)} %slice.32), channel_id=1, source_target_pairs={{0,4},{4,8},{8,12},{12,16},{16,20},{20,24},{24,28},{28,32},{32,36}... | collective-permute-start | bytes 1572872 | tf_op jit(solution)/shard_map/ppermute | solution.py:27
  53.0 10.0 %copy-start.1 = (bf16[2,8,48,512]{3,2,1,0:T(8,128)(2,1)}, bf16[2,8,48,512]{3,2,1,0:T(8,128)(2,1)S(1)}, u32[]{:S(2)}) copy-start(bf16[2,8,48,512]{3,2,1,0:T(8,128)(2,1)S(1)} %collective-permute-done.11.refs_5_) | copy-start | bytes 2359300
  53.0 12.5 %collective-permute-start.5 = (bf16[2,8,32,512]{3,2,1,0:T(8,128)(2,1)}, bf16[2,8,32,512]{3,2,1,0:T(8,128)(2,1)}, u32[]{:S(2)}, u32[]{:S(2)}) collective-permute-start(bf16[2,8,32,512]{3,2,1,0:T(8,128)(2,1)} %slice.33), channel_id=1, source_target_pairs={{4,0},{8,4},{12,8},{16,12},{20,16},{24,20},{28,24},{32,28},{36,32}... | collective-permute-start | bytes 1572872 | tf_op jit(solution)/shard_map/ppermute | solution.py:27
  54.9 8.1 %copy-start.2 = (bf16[2,8,48,512]{3,2,1,0:T(8,128)(2,1)}, bf16[2,8,48,512]{3,2,1,0:T(8,128)(2,1)S(1)}, u32[]{:S(2)}) copy-start(bf16[2,8,48,512]{3,2,1,0:T(8,128)(2,1)S(1)} %collective-permute-done.12.refs_6_) | copy-start | bytes 2359300
  54.9 38.9 %collective-permute-start.10 = (bf16[2,8,48,512]{3,2,1,0:T(8,128)(2,1)}, bf16[2,8,48,512]{3,2,1,0:T(8,128)(2,1)}, u32[]{:S(2)}, u32[]{:S(2)}) collective-permute-start(bf16[2,8,48,512]{3,2,1,0:T(8,128)(2,1)} %shard_map.81.refs_2_), channel_id=1, source_target_pairs={{0,4},{4,0},{8,12},{12,8},{16,20},{20,16},{24,28},{28,24},{32,36},... | collective-permute-start | bytes 2359304 | tf_op jit(solution)/shard_map/ppermute | solution.py:36
  55.6 39.9 %collective-permute-start.13 = (bf16[2,8,48,512]{3,2,1,0:T(8,128)(2,1)S(1)}, bf16[2,8,48,512]{3,2,1,0:T(8,128)(2,1)}, u32[]{:S(2)}, u32[]{:S(2)}) collective-permute-start(bf16[2,8,48,512]{3,2,1,0:T(8,128)(2,1)S(1)} %broadcast_select_fusion), channel_id=1, source_target_pairs={{0,4},{4,0},{8,12},{12,8},{16,20},{20,16},{24,28},{28,24},{32,36},... | collective-permute-start | bytes 2359304 | tf_op jit(solution)/shard_map/ppermute | solution.py:36
  63.1 32.4 %collective-permute-start.14 = (bf16[2,8,32,512]{3,2,1,0:T(8,128)(2,1)S(1)}, bf16[2,8,32,512]{3,2,1,0:T(8,128)(2,1)S(1)}, u32[]{:S(2)}, u32[]{:S(2)}) collective-permute-start(bf16[2,8,32,512]{3,2,1,0:T(8,128)(2,1)S(1)} %slice.36), channel_id=1, source_target_pairs={{0,4},{4,8},{8,12},{12,16},{16,20},{20,24},{24,28},{28,32},{32,36}... | collective-permute-start | bytes 1572872 | tf_op jit(solution)/shard_map/ppermute | solution.py:27
  65.5 30.0 %collective-permute-start.15 = (bf16[2,8,32,512]{3,2,1,0:T(8,128)(2,1)S(1)}, bf16[2,8,32,512]{3,2,1,0:T(8,128)(2,1)}, u32[]{:S(2)}, u32[]{:S(2)}) collective-permute-start(bf16[2,8,32,512]{3,2,1,0:T(8,128)(2,1)S(1)} %slice.37), channel_id=1, source_target_pairs={{4,0},{8,4},{12,8},{16,12},{20,16},{24,20},{28,24},{32,28},{36,32}... | collective-permute-start | bytes 1572872 | tf_op jit(solution)/shard_map/ppermute | solution.py:27
  92.3 26.8 %collective-permute-start.6 = (bf16[2,384,256]{2,1,0:T(8,128)(2,1)}, bf16[2,384,256]{2,1,0:T(8,128)(2,1)S(1)}, u32[]{:S(2)}, u32[]{:S(2)}) collective-permute-start(bf16[2,384,256]{2,1,0:T(8,128)(2,1)} %get-tuple-element.6.refs_1_), channel_id=1, source_target_pairs={{0,1},{1,2},{2,3},{3,0},{4,5},{5,6},{6,7},{7,4},{8,9},{9,10},{10,1... | collective-permute-start | bytes 1179656 | tf_op jit(solution)/shard_map/ppermute | solution.py:32
  93.8 25.7 %collective-permute-start.7 = (bf16[2,384,256]{2,1,0:T(8,128)(2,1)}, bf16[2,384,256]{2,1,0:T(8,128)(2,1)S(1)}, u32[]{:S(2)}, u32[]{:S(2)}) collective-permute-start(bf16[2,384,256]{2,1,0:T(8,128)(2,1)} %get-tuple-element.6.refs_1_), channel_id=1, source_target_pairs={{0,3},{1,0},{2,1},{3,2},{4,7},{5,4},{6,5},{7,6},{8,11},{9,8},{10,9... | collective-permute-start | bytes 1179656 | tf_op jit(solution)/shard_map/ppermute | solution.py:32
  95.5 0.8 copy-start.15
  115.8 15.5 %copy-start.13 = (f32[2,2,384]{2,1,0:T(2,128)S(1)}, f32[2,2,384]{2,1,0:T(2,128)}, u32[]{:S(2)}) copy-start(f32[2,2,384]{2,1,0:T(2,128)} %get-tuple-element.8) | copy-start | bytes 18436
  115.8 15.5 %copy-start.14 = (f32[2,2,384]{2,1,0:T(2,128)S(1)}, f32[2,2,384]{2,1,0:T(2,128)}, u32[]{:S(2)}) copy-start(f32[2,2,384]{2,1,0:T(2,128)} %get-tuple-element.9) | copy-start | bytes 18436
  115.8 12.1 %collective-permute-start.16 = (bf16[2,384,256]{2,1,0:T(8,128)(2,1)}, bf16[2,384,256]{2,1,0:T(8,128)(2,1)S(1)}, u32[]{:S(2)}, u32[]{:S(2)}) collective-permute-start(bf16[2,384,256]{2,1,0:T(8,128)(2,1)} %get-tuple-element.7.refs_1_), channel_id=1, source_target_pairs={{0,1},{1,2},{2,3},{3,0},{4,5},{5,6},{6,7},{7,4},{8,9},{9,10},{10,1... | collective-permute-start | bytes 1179656 | tf_op jit(solution)/shard_map/ppermute | solution.py:32
  116.2 11.8 %collective-permute-start.17 = (bf16[2,384,256]{2,1,0:T(8,128)(2,1)}, bf16[2,384,256]{2,1,0:T(8,128)(2,1)S(1)}, u32[]{:S(2)}, u32[]{:S(2)}) collective-permute-start(bf16[2,384,256]{2,1,0:T(8,128)(2,1)} %get-tuple-element.7.refs_1_), channel_id=1, source_target_pairs={{0,3},{1,0},{2,1},{3,2},{4,7},{5,4},{6,5},{7,6},{8,11},{9,8},{10,9... | collective-permute-start | bytes 1179656 | tf_op jit(solution)/shard_map/ppermute | solution.py:32
  119.1 12.8 %copy-start.5 = (bf16[2,384,256]{2,1,0:T(8,128)(2,1)}, bf16[2,384,256]{2,1,0:T(8,128)(2,1)S(1)}, u32[]{:S(2)}) copy-start(bf16[2,384,256]{2,1,0:T(8,128)(2,1)S(1)} %collective-permute-done.6.refs_2_) | copy-start | bytes 1179652
  119.2 12.8 %collective-permute-start.8 = (bf16[2,192,256]{2,1,0:T(8,128)(2,1)S(1)}, bf16[2,192,256]{2,1,0:T(8,128)(2,1)S(1)}, u32[]{:S(2)}, u32[]{:S(2)}) collective-permute-start(bf16[2,192,256]{2,1,0:T(8,128)(2,1)S(1)} %slice.34), channel_id=1, source_target_pairs={{0,1},{1,2},{2,3},{3,0},{4,5},{5,6},{6,7},{7,4},{8,9},{9,10},{10,1... | collective-permute-start | bytes 589832 | tf_op jit(solution)/shard_map/ppermute | solution.py:32
  119.5 12.5 %copy-start.6 = (bf16[2,384,256]{2,1,0:T(8,128)(2,1)}, bf16[2,384,256]{2,1,0:T(8,128)(2,1)S(1)}, u32[]{:S(2)}) copy-start(bf16[2,384,256]{2,1,0:T(8,128)(2,1)S(1)} %collective-permute-done.7.refs_3_) | copy-start | bytes 1179652
  119.5 12.5 %collective-permute-start.9 = (bf16[2,192,256]{2,1,0:T(8,128)(2,1)S(1)}, bf16[2,192,256]{2,1,0:T(8,128)(2,1)S(1)}, u32[]{:S(2)}, u32[]{:S(2)}) collective-permute-start(bf16[2,192,256]{2,1,0:T(8,128)(2,1)S(1)} %slice.35), channel_id=1, source_target_pairs={{0,3},{1,0},{2,1},{3,2},{4,7},{5,4},{6,5},{7,6},{8,11},{9,8},{10,9... | collective-permute-start | bytes 589832 | tf_op jit(solution)/shard_map/ppermute | solution.py:32
  127.9 9.9 %copy-start.7 = (bf16[2,384,256]{2,1,0:T(8,128)(2,1)}, bf16[2,384,256]{2,1,0:T(8,128)(2,1)S(1)}, u32[]{:S(2)}) copy-start(bf16[2,384,256]{2,1,0:T(8,128)(2,1)S(1)} %collective-permute-done.16.refs_2_) | copy-start | bytes 1179652
  127.9 9.9 %collective-permute-start.18 = (bf16[2,192,256]{2,1,0:T(8,128)(2,1)S(1)}, bf16[2,192,256]{2,1,0:T(8,128)(2,1)S(1)}, u32[]{:S(2)}, u32[]{:S(2)}) collective-permute-start(bf16[2,192,256]{2,1,0:T(8,128)(2,1)S(1)} %slice.38), channel_id=1, source_target_pairs={{0,1},{1,2},{2,3},{3,0},{4,5},{5,6},{6,7},{7,4},{8,9},{9,10},{10,1... | collective-permute-start | bytes 589832 | tf_op jit(solution)/shard_map/ppermute | solution.py:32
  128.0 9.8 %copy-start.8 = (bf16[2,384,256]{2,1,0:T(8,128)(2,1)}, bf16[2,384,256]{2,1,0:T(8,128)(2,1)S(1)}, u32[]{:S(2)}) copy-start(bf16[2,384,256]{2,1,0:T(8,128)(2,1)S(1)} %collective-permute-done.17.refs_3_) | copy-start | bytes 1179652
  128.1 9.8 %collective-permute-start.19 = (bf16[2,192,256]{2,1,0:T(8,128)(2,1)S(1)}, bf16[2,192,256]{2,1,0:T(8,128)(2,1)S(1)}, u32[]{:S(2)}, u32[]{:S(2)}) collective-permute-start(bf16[2,192,256]{2,1,0:T(8,128)(2,1)S(1)} %slice.39), channel_id=1, source_target_pairs={{0,3},{1,0},{2,1},{3,2},{4,7},{5,4},{6,5},{7,6},{8,11},{9,8},{10,9... | collective-permute-start | bytes 589832 | tf_op jit(solution)/shard_map/ppermute | solution.py:32
  132.0 0.7 copy-start.9
  132.0 0.7 copy-start.11
  137.8 6.5 %copy-start = (bf16[2,384,512]{2,1,0:T(8,128)(2,1)S(1)}, bf16[2,384,512]{2,1,0:T(8,128)(2,1)}, u32[]{:S(2)}) copy-start(bf16[2,384,512]{2,1,0:T(8,128)(2,1)} %shard_map.80) | copy-start | bytes 2359300
  137.8 0.7 copy-start.10
  138.5 0.7 copy-start.12
where the time goes:
time: 147 us
  Pallas kernels  72 us (49%)
  starting transfers between devices  46 us (31%)
  waiting for transfers between devices  16.4 us (11%)
  other arithmetic  6.56 us (4%)
  local copies, waits for them, and re-layouts  4.72 us (3%)
    pallas_call x2, Pallas kernels, attend(): pl.pallas_call(lambda *refs: attend_body(blocks, *refs), grid_spec=pltpu....  39 us
    ppermute x8, starting transfers between devices, shifted(): lax.ppermute(block, axis, [(i - distance, i) for i in devices if i - dist...  31.4 us
    pallas_call x3, Pallas kernels, project(): pl.pallas_call(lambda *refs: project_body(turns, *refs), grid=(count,), i...  22.9 us
    ppermute x8, starting transfers between devices, turned(): lax.ppermute(block, axis, [(i, (i + distance) % size) for i in range(size)])  13.5 us
    ppermute x8, waiting for transfers between devices, shifted(): lax.ppermute(block, axis, [(i - distance, i) for i in devices if i - dist...  11.2 us
    pallas_call x2, Pallas kernels, finish(): pl.pallas_call(lambda *refs: finish_body(channels_all, *refs), grid_spec=...  10.2 us
    ppermute x8, waiting for transfers between devices, turned(): lax.ppermute(block, axis, [(i, (i + distance) % size) for i in range(size)])  5.13 us
  transfers between devices with their start and end apart: 20, of which 3 were waited for; matrix products, arithmetic and copies ran while one was open for 3% of the time, Pallas kernels for 40%

commit v1 on v0

--- a/solution.py
+++ b/solution.py
@@ -51,54 +51,66 @@
     return jnp.concatenate(heads, axis=1)
 
 
-def project_body(turns, tokens_ref, cos_ref, sin_ref, *refs):
-    weights, out_ref, order_ref = refs[: len(turns)], refs[-2], refs[-1]
-    length = tokens_ref.shape[1]
+PIECES = 2
+
+
+def project_body(*refs):
+    pieces, refs = refs[:PIECES], refs[PIECES:]
+    cos_ref, sin_ref, query_ref, key_ref, value_ref, q_ref, kv_ref, order_ref = refs
+    length = cos_ref.shape[0]
+    width = query_ref.shape[1]
 
     @pl.when(pl.program_id(0) == 0)
     def _():
         order_ref[...] = row_order(length, jnp.bfloat16)
 
-    rows = tokens_ref[0]
-    at = 0
-    for turn, weight in zip(turns, weights):
-        made = jnp.dot(rows, weight[...], preferred_element_type=jnp.float32)
-        if turn:
-            made = rotated(made, cos_ref[...], sin_ref[...])
-        width = made.shape[1]
-        moved = jnp.dot(order_ref[...], made.astype(jnp.bfloat16), preferred_element_type=jnp.float32)
-        moved = moved.astype(jnp.bfloat16).reshape(CLASSES, length // CLASSES, width)
-        out_ref[0, :, :, at : at + width] = moved
-        at += width
-
-
-def project(tokens, first, count, cosine, sine, weights, turns):
+    def made(weight):
+        return jnp.concatenate(
+            [jnp.dot(p[0], weight[...], preferred_element_type=jnp.float32) for p in pieces], axis=0
+        )
+
+    def moved(value):
+        value = jnp.dot(order_ref[...], value.astype(jnp.bfloat16), preferred_element_type=jnp.float32)
+        return value.astype(jnp.bfloat16).reshape(CLASSES, length // CLASSES, width)
+
+    keys = made(key_ref)
+    values = made(value_ref)
+    queries = made(query_ref)
+    kv_ref[0, :, :, :width] = moved(rotated(keys, cos_ref[...], sin_ref[...]))
+    kv_ref[0, :, :, width:] = moved(values)
+    q_ref[0] = moved(rotated(queries, cos_ref[...], sin_ref[...]))
+
+
+def project(tokens, first, count, cosine, sine, query_weight, key_weight, value_weight):
     _, length, model_dim = tokens.shape
-    width = sum(w.shape[1] for w in weights)
+    width = query_weight.shape[1]
+    weights = (query_weight, key_weight, value_weight)
+    rows = length // PIECES
     whole = lambda a: pl.BlockSpec(a.shape, lambda s: (0,) * a.ndim)
+    made = lambda wide: pl.BlockSpec((1, CLASSES, length // CLASSES, wide), lambda s: (s, 0, 0, 0))
+    piece = lambda n: pl.BlockSpec((1, rows, model_dim), lambda s: (s + first, n, 0))
     return pl.pallas_call(
-        lambda *refs: project_body(turns, *refs),
+        project_body,
         grid=(count,),
-        in_specs=[
-            pl.BlockSpec((1, length, model_dim), lambda s: (s + first, 0, 0)),
-            whole(cosine),
-            whole(sine),
-            *[whole(w) for w in weights],
+        in_specs=[*map(piece, range(PIECES)), whole(cosine), whole(sine), *[whole(w) for w in weights]],
+        out_specs=[made(width), made(2 * width)],
+        out_shape=[
+            jax.ShapeDtypeStruct((count, CLASSES, length // CLASSES, wide), jnp.bfloat16)
+            for wide in (width, 2 * width)
         ],
-        out_specs=pl.BlockSpec((1, CLASSES, length // CLASSES, width), lambda s: (s, 0, 0, 0)),
-        out_shape=jax.ShapeDtypeStruct((count, CLASSES, length // CLASSES, width), jnp.bfloat16),
         scratch_shapes=[pltpu.VMEM((length, length), jnp.bfloat16)],
         cost_estimate=pl.CostEstimate(
-            flops=2 * count * length * model_dim * width,
+            flops=6 * count * length * model_dim * width,
             transcendentals=0,
-            bytes_accessed=2 * (count * length * (model_dim + width) + model_dim * width),
-        ),
-    )(tokens, cosine, sine, *weights)
+            bytes_accessed=2 * (count * length * (model_dim + 3 * width) + 3 * model_dim * width),
+        ),
+    )(*[tokens] * PIECES, cosine, sine, *weights)
 
 
 def attend_body(
     blocks, place_ref, q_ref, own_ref, first_ref, second_ref, left2_ref, right2_ref, left3_ref, right3_ref,
-    out_ref, log_ref, left1, right1, far_bias, near_bias, unit_bias, acc, peak, total, logs, order
+    out_ref, log_ref, left1, right1, far_bias, near_bias, unit_bias,
+    raw_unit, raw_near, raw_far, probs_unit, probs_near, probs_far, acc, peak, total, logs, order
 ):
     per = q_ref.shape[2]
     channels = q_ref.shape[3]
@@ -109,6 +121,8 @@
     start = place_ref[0] * per
     limit = blocks * per
     south = place_ref[1]
+    raw = (raw_unit, raw_near, raw_far)
+    probs = (probs_unit, probs_near, probs_far)
 
     @pl.when(pl.program_id(0) == 0)
     def _():
@@ -146,89 +160,101 @@
     left1[...] = jnp.where(south == 1, second_ref[0], first_ref[0])
     right1[...] = jnp.where(south == 1, first_ref[0], second_ref[0])
 
-    def soft(q, k, v, bias):
-        scores = lax.dot_general(q, k, (((1,), (1,)), ((), ())), preferred_element_type=jnp.float32) + bias
+    half = CLASSES // 2
+    slabs = per // tile
+
+    def near_unit(lanes, t):
+        lo, hi = tile * (t - 1), tile * (t + 2)
+        parts = []
+        if lo < 0:
+            parts.append(left1[:, per + lo : per, lanes])
+        parts.append(own_ref[0, :, max(lo, 0) : min(hi, per), lanes])
+        if hi > per:
+            parts.append(right1[:, 0 : hi - per, lanes])
+        joined = jnp.concatenate(parts, axis=1) if len(parts) > 1 else parts[0]
+        return joined.reshape(CLASSES * 3 * tile, HEAD_DIM)
+
+    def near_pair(lanes, c):
+        parts = []
+        for r in (c, c + half):
+            parts += [left1[r, per - reach_near : per, lanes], own_ref[0, r, :, lanes], right1[r, 0:reach_near, lanes]]
+        return jnp.concatenate(parts, axis=0)
+
+    def near_far(lanes, r):
+        parts = [left3_ref[0, r, :, lanes], left2_ref[0, r, :, lanes], left1[r, :, lanes], own_ref[0, r, :, lanes]]
+        parts += [right1[r, :, lanes], right2_ref[0, r, :, lanes], right3_ref[0, r, :, lanes]]
+        return jnp.concatenate(parts, axis=0)
+
+    keys_of = (near_unit, near_pair, near_far)
+
+    def queries_of(kind, lanes, b):
+        if kind == 0:
+            return q_ref[0, :, b * tile : (b + 1) * tile, lanes].reshape(CLASSES * tile, HEAD_DIM)
+        if kind == 1:
+            return jnp.concatenate([q_ref[0, b, :, lanes], q_ref[0, b + half, :, lanes]], axis=0)
+        return q_ref[0, b, :, lanes]
+
+    def bias_of(kind, b):
+        return (unit_bias, near_bias, far_bias)[kind][b] if kind == 0 else (near_bias, far_bias)[kind - 1][...]
+
+    def score(h, kind, b):
+        lanes = slice(h * HEAD_DIM, (h + 1) * HEAD_DIM)
+        made = lax.dot_general(
+            queries_of(kind, lanes, b), keys_of[kind](lanes, b), (((1,), (1,)), ((), ())),
+            preferred_element_type=jnp.float32,
+        )
+        raw[kind][h, b] = made + bias_of(kind, b)
+
+    def weigh(h, kind, b):
+        scores = raw[kind][h, b]
         top = jnp.max(scores, axis=1, keepdims=True)
         weights = jnp.exp2((scores - top) * EXP2_SCALE)
         weight_sum = jnp.sum(weights, axis=1, keepdims=True)
-        summed = jnp.dot(weights.astype(jnp.bfloat16), v, preferred_element_type=jnp.float32)
-        return top, weight_sum, summed
-
+        probs[kind][h, b] = weights.astype(jnp.bfloat16)
+        rows = scores.shape[0]
+        put(peak, h, kind, b, jnp.broadcast_to(top, (rows, HEAD_DIM)))
+        put(total, h, kind, b, jnp.broadcast_to(weight_sum, (rows, HEAD_DIM)))
+
+    def put(ref, h, kind, b, value):
+        if kind == 0:
+            ref[h, 0, :, b * tile : (b + 1) * tile, :] = value.reshape(CLASSES, tile, HEAD_DIM)
+        elif kind == 1:
+            ref[h, 1, b] = value[:per]
+            ref[h, 1, b + half] = value[per:]
+        else:
+            ref[h, 2, b] = value
+
+    def blend(h, kind, b):
+        lanes = slice(channels + h * HEAD_DIM, channels + (h + 1) * HEAD_DIM)
+        summed = jnp.dot(probs[kind][h, b], keys_of[kind](lanes, b), preferred_element_type=jnp.float32)
+        if kind < 2:
+            put(acc, h, kind, b, summed)
+            return
+        tops = [peak[h, k, b] for k in range(3)]
+        new = jnp.maximum(jnp.maximum(tops[0], tops[1]), tops[2])
+        shares = [jnp.exp2((top - new) * EXP2_SCALE) for top in tops]
+        whole = total[h, 0, b] * shares[0] + total[h, 1, b] * shares[1] + total[h, 2, b] * shares[2]
+        value = acc[h, 0, b] * shares[0] + acc[h, 1, b] * shares[1] + summed * shares[2]
+        rows = slice(b * per, (b + 1) * per)
+        out_ref[0, rows, h * HEAD_DIM : (h + 1) * HEAD_DIM] = (value / whole).astype(jnp.bfloat16)
+        log = new * SCALE + jnp.log(whole)
+        if h == 0:
+            logs[rows] = log
+        else:
+            lane = lax.broadcasted_iota(jnp.int32, (per, HEAD_DIM), 1)
+            logs[rows] = jnp.where(lane == h, log, logs[rows])
+
+    units = []
     for h in range(heads):
-        ql = slice(h * HEAD_DIM, (h + 1) * HEAD_DIM)
-        kl = ql
-        vl = slice(channels + h * HEAD_DIM, channels + (h + 1) * HEAD_DIM)
-        blocks_of = per // tile
-        for t in range(blocks_of):
-            here = slice(t * tile, (t + 1) * tile)
-            lo, hi = tile * (t - 1), tile * (t + 2)
-
-            def around(lanes):
-                parts = []
-                if lo < 0:
-                    parts.append(left1[:, per + lo : per, lanes])
-                parts.append(own_ref[0, :, max(lo, 0) : min(hi, per), lanes])
-                if hi > per:
-                    parts.append(right1[:, 0 : hi - per, lanes])
-                joined = jnp.concatenate(parts, axis=1) if len(parts) > 1 else parts[0]
-                return joined.reshape(CLASSES * 3 * tile, HEAD_DIM)
-
-            q = q_ref[0, :, here, ql].reshape(CLASSES * tile, HEAD_DIM)
-            top, weight_sum, summed = soft(q, around(kl), around(vl), unit_bias[t])
-            dims = (CLASSES, tile, HEAD_DIM)
-            acc[:, here, :] = summed.reshape(dims)
-            peak[:, here, :] = jnp.broadcast_to(top, (CLASSES * tile, HEAD_DIM)).reshape(dims)
-            total[:, here, :] = jnp.broadcast_to(weight_sum, (CLASSES * tile, HEAD_DIM)).reshape(dims)
-        half = CLASSES // 2
-        for c in range(half):
-
-            def around(lanes):
-                parts = []
-                for r in (c, c + half):
-                    parts += [left1[r, per - reach_near : per, lanes], own_ref[0, r, :, lanes], right1[r, 0:reach_near, lanes]]
-                return jnp.concatenate(parts, axis=0)
-
-            q = jnp.concatenate([q_ref[0, c, :, ql], q_ref[0, c + half, :, ql]], axis=0)
-            top, weight_sum, summed = soft(q, around(kl), around(vl), near_bias[...])
-            for n, r in enumerate((c, c + half)):
-                rows = slice(n * per, (n + 1) * per)
-                old = peak[r]
-                new = jnp.maximum(old, top[rows])
-                keep = jnp.exp2((old - new) * EXP2_SCALE)
-                add = jnp.exp2((top[rows] - new) * EXP2_SCALE)
-                acc[r] = acc[r] * keep + summed[rows] * add
-                total[r] = total[r] * keep + weight_sum[rows] * add
-                peak[r] = new
-        for r in range(CLASSES):
-
-            def around(lanes):
-                return jnp.concatenate(
-                    [
-                        left3_ref[0, r, :, lanes],
-                        left2_ref[0, r, :, lanes],
-                        left1[r, :, lanes],
-                        own_ref[0, r, :, lanes],
-                        right1[r, :, lanes],
-                        right2_ref[0, r, :, lanes],
-                        right3_ref[0, r, :, lanes],
-                    ],
-                    axis=0,
-                )
-
-            top, weight_sum, summed = soft(q_ref[0, r, :, ql], around(kl), around(vl), far_bias[...])
-            old = peak[r]
-            new = jnp.maximum(old, top)
-            keep = jnp.exp2((old - new) * EXP2_SCALE)
-            add = jnp.exp2((top - new) * EXP2_SCALE)
-            whole = total[r] * keep + weight_sum * add
-            out_ref[0, r * per : (r + 1) * per, ql] = ((acc[r] * keep + summed * add) / whole).astype(jnp.bfloat16)
-            log = new * SCALE + jnp.log(whole)
-            rows = slice(r * per, (r + 1) * per)
-            if h == 0:
-                logs[rows] = log
-            else:
-                lane = lax.broadcasted_iota(jnp.int32, (per, HEAD_DIM), 1)
-                logs[rows] = jnp.where(lane == h, log, logs[rows])
+        units.append([(h, 0, t) for t in range(slabs)])
+        units.append([(h, 1, c) for c in range(half)])
+        units.append([(h, 2, r) for r in range(half)])
+        units.append([(h, 2, r) for r in range(half, CLASSES)])
+    for step in range(len(units) + 2):
+        for stage, lag in ((score, 0), (blend, 2), (weigh, 1)):
+            if 0 <= step - lag < len(units):
+                for item in units[step - lag]:
+                    stage(*item)
     left = logs[...]
     natural = jnp.zeros((HEAD_DIM, CLASSES * per), jnp.float32)
     for _ in range(3):
@@ -238,7 +264,7 @@
     log_ref[0] = natural[0:heads]
 
 
-def attend(place, blocks, q, first, own, swap_own, swap_far, left2, right2, left3, right3):
+def attend(place, blocks, q, own, swap_own, swap_far, left2, right2, left3, right3):
     count, classes, per, both = own.shape
     channels = both // 2
     heads = channels // HEAD_DIM
@@ -250,13 +276,18 @@
     f32 = jnp.float32
     far_keys = per + 2 * REACH * FAR // CLASSES
     near_keys = 2 * (per + 2 * reach_near)
+    blocks_of = (
+        (heads, per // 16, classes * 16, classes * 48),
+        (heads, classes // 2, 2 * per, near_keys),
+        (heads, classes, per, far_keys),
+    )
     return pl.pallas_call(
         lambda *refs: attend_body(blocks, *refs),
         grid_spec=pltpu.PrefetchScalarGridSpec(
             num_scalar_prefetch=1,
             grid=(count,),
             in_specs=[
-                pl.BlockSpec((1, classes, per, channels), lambda s, p: (s + first, 0, 0, 0)),
+                pl.BlockSpec((1, classes, per, channels), lambda s, p: (s, 0, 0, 0)),
                 whole, whole, whole, whole, whole, part, part,
             ],
             out_specs=[
@@ -269,9 +300,10 @@
                 pltpu.VMEM((per, far_keys), f32),
                 pltpu.VMEM((2 * per, near_keys), f32),
                 pltpu.VMEM((per // 16, classes * 16, classes * 48), f32),
-                pltpu.VMEM((classes, per, HEAD_DIM), f32),
-                pltpu.VMEM((classes, per, HEAD_DIM), f32),
-                pltpu.VMEM((classes, per, HEAD_DIM), f32),
+                *[pltpu.VMEM(dims, dtype) for dtype in (f32, jnp.bfloat16) for dims in blocks_of],
+                pltpu.VMEM((heads, 2, classes, per, HEAD_DIM), f32),
+                pltpu.VMEM((heads, 3, classes, per, HEAD_DIM), f32),
+                pltpu.VMEM((heads, 3, classes, per, HEAD_DIM), f32),
                 pltpu.VMEM((length, HEAD_DIM), f32),
                 pltpu.VMEM((length, length), jnp.bfloat16),
             ],
@@ -369,19 +401,18 @@
     first = 0
     stage = []
     for count in CHUNKS:
-        own = project(tokens, first, count, cosine, sine, (key_weight, value_weight), (True, False))
+        queries, own = project(tokens, first, count, cosine, sine, query_weight, key_weight, value_weight)
         left2 = shifted(own, "sp", 2)
         right2 = shifted(own, "sp", -2)
         swap_own = swapped(own, "sp")
-        stage.append((first, count, own, left2, right2, swap_own))
+        stage.append((queries, own, left2, right2, swap_own))
         first += count
-    queries = project(tokens, 0, seq_count, cosine, sine, (query_weight,), (True,))
-    for first, count, own, left2, right2, swap_own in stage:
+    for queries, own, left2, right2, swap_own in stage:
         swap_far = swapped(jnp.where(core == 1, left2, right2), "sp")
         left3 = shifted(left2[:, :, per - edge :], "sp", 1)
         right3 = shifted(right2[:, :, :edge], "sp", -1)
         merged, logs = attend(
-            place, blocks, queries, first, own, swap_own, swap_far, left2, right2, left3, right3
+            place, blocks, queries, own, swap_own, swap_far, left2, right2, left3, right3
         )
         before = turned(merged, "tp", 1)
         after = turned(merged, "tp", -1)

time: 147 us -> 119 us (0.81)
  Pallas kernels: 72 us -> 39.8 us
  waiting for transfers between devices: 16.4 us -> 21 us
    pallas_call x2, Pallas kernels: 39 us -> 15.8 us  [attend(): pl.pallas_call(lambda *refs: attend_body(blocks, *refs), grid_spec=pltpu....]
    pallas_call x3 -> x2, Pallas kernels: 22.9 us -> 13.8 us  [project(): pl.pallas_call(project_body, grid=(count,), in_specs=[*map(piece, range(P...]
    ppermute x8, waiting for transfers between devices: 11.2 us -> 16.2 us  [shifted(): lax.ppermute(block, axis, [(i - distance, i) for i in devices if i - dist...]
  transfers between devices with their start and end apart: 20 -> 20, of which waited for: 3 -> 6; matrix products, arithmetic and copies ran while one was open for 3% -> 4% of each run, Pallas kernels for 40% -> 23%
where the time goes in v1:
time: 119 us
  starting transfers between devices  45.7 us (38%)
  Pallas kernels  39.8 us (33%)
  waiting for transfers between devices  21 us (18%)
  other arithmetic  6.5 us (5%)
  local copies, waits for them, and re-layouts  4.72 us (4%)
    ppermute x8, starting transfers between devices, shifted(): lax.ppermute(block, axis, [(i - distance, i) for i in devices if i - dist...  31.6 us
    ppermute x8, waiting for transfers between devices, shifted(): lax.ppermute(block, axis, [(i - distance, i) for i in devices if i - dist...  16.2 us
    pallas_call x2, Pallas kernels, attend(): pl.pallas_call(lambda *refs: attend_body(blocks, *refs), grid_spec=pltpu....  15.8 us
    pallas_call x2, Pallas kernels, project(): pl.pallas_call(project_body, grid=(count,), in_specs=[*map(piece, range(P...  13.8 us
    ppermute x8, starting transfers between devices, turned(): lax.ppermute(block, axis, [(i, (i + distance) % size) for i in range(size)])  13.3 us
    pallas_call x2, Pallas kernels, finish(): pl.pallas_call(lambda *refs: finish_body(channels_all, *refs), grid_spec=...  10.2 us
    ppermute x8, waiting for transfers between devices, turned(): lax.ppermute(block, axis, [(i, (i + distance) % size) for i in range(size)])  4.77 us
    unnamed x32, local copies, waits for them, and re-layouts  2.88 us
  transfers between devices with their start and end apart: 20, of which 6 were waited for; matrix products, arithmetic and copies ran while one was open for 4% of the time, Pallas kernels for 23%

profile of v1, /device:TPU:128, one launch (start us, length us, event | category | flops | bytes accessed | tf_op | source)
XLA Modules:
  0.0 118.7 jit_solution(11868705558825688215)
XLA Ops:
  0.7 0.8 fusion
  1.4 0.9 pad_maximum_fusion.1
  2.4 6.9 %shard_map.77 = (bf16[2,8,48,256]{3,2,1,0:T(8,128)(2,1)}, bf16[2,8,48,512]{3,2,1,0:T(8,128)(2,1)}) custom-call(bf16[4,384,2048]{2,1,0:T(8,128)(2,1)} %refs_1_.3, bf16[4,384,2048]{2,1,0:T(8,128)(2,1)} %refs_1_.3, f32[384,128]{1,0:T(8,128)} %get-tuple-element.21.refs_2_, f32[384,128]{1,0:T(8,128)} %get-tuple-element.22.refs_3_, bf16[2048,256]{1,0:T(8,128)(2,1)} %refs_4_.3, ...), custom_call_target="tpu_custom_call" | custom-call | flops 2415919104 | bytes 7471104 | tf_op jit(solution)/shard_map/pallas_call | solution.py:92
  9.3 3.5 %collective-permute-start.1 = (bf16[2,8,48,512]{3,2,1,0:T(8,128)(2,1)}, bf16[2,8,48,512]{3,2,1,0:T(8,128)(2,1)S(1)}, u32[]{:S(2)}, u32[]{:S(2)}) collective-permute-start(bf16[2,8,48,512]{3,2,1,0:T(8,128)(2,1)} %get-tuple-element.11.refs_2_), channel_id=1, source_target_pairs={{0,8},{4,12},{8,16},{12,20},{16,24},{20,28},{24,32},{28,36},{32,40... | collective-permute-start | bytes 2359304 | tf_op jit(solution)/shard_map/ppermute | solution.py:27
  12.7 5.7 %collective-permute-start.2 = (bf16[2,8,48,512]{3,2,1,0:T(8,128)(2,1)}, bf16[2,8,48,512]{3,2,1,0:T(8,128)(2,1)S(1)}, u32[]{:S(2)}, u32[]{:S(2)}) collective-permute-start(bf16[2,8,48,512]{3,2,1,0:T(8,128)(2,1)} %get-tuple-element.11.refs_2_), channel_id=1, source_target_pairs={{8,0},{12,4},{16,8},{20,12},{24,16},{28,20},{32,24},{36,28},{40,32... | collective-permute-start | bytes 2359304 | tf_op jit(solution)/shard_map/ppermute | solution.py:27
  18.4 6.9 %shard_map.80 = (bf16[2,8,48,256]{3,2,1,0:T(8,128)(2,1)}, bf16[2,8,48,512]{3,2,1,0:T(8,128)(2,1)}) custom-call(bf16[4,384,2048]{2,1,0:T(8,128)(2,1)} %refs_1_.3, bf16[4,384,2048]{2,1,0:T(8,128)(2,1)} %refs_1_.3, f32[384,128]{1,0:T(8,128)} %get-tuple-element.21.refs_2_, f32[384,128]{1,0:T(8,128)} %get-tuple-element.22.refs_3_, bf16[2048,256]{1,0:T(8,128)(2,1)} %refs_4_.3, ...), custom_call_target="tpu_custom_call" | custom-call | flops 2415919104 | bytes 7471104 | tf_op jit(solution)/shard_map/pallas_call | solution.py:92
  25.3 1.9 %collective-permute-start.11 = (bf16[2,8,48,512]{3,2,1,0:T(8,128)(2,1)}, bf16[2,8,48,512]{3,2,1,0:T(8,128)(2,1)S(1)}, u32[]{:S(2)}, u32[]{:S(2)}) collective-permute-start(bf16[2,8,48,512]{3,2,1,0:T(8,128)(2,1)} %get-tuple-element.14.refs_2_), channel_id=1, source_target_pairs={{0,8},{4,12},{8,16},{12,20},{16,24},{20,28},{24,32},{28,36},{32,40... | collective-permute-start | bytes 2359304 | tf_op jit(solution)/shard_map/ppermute | solution.py:27
  27.3 7.2 %collective-permute-start.12 = (bf16[2,8,48,512]{3,2,1,0:T(8,128)(2,1)}, bf16[2,8,48,512]{3,2,1,0:T(8,128)(2,1)S(1)}, u32[]{:S(2)}, u32[]{:S(2)}) collective-permute-start(bf16[2,8,48,512]{3,2,1,0:T(8,128)(2,1)} %get-tuple-element.14.refs_2_), channel_id=1, source_target_pairs={{8,0},{12,4},{16,8},{20,12},{24,16},{28,20},{32,24},{36,28},{40,32... | collective-permute-start | bytes 2359304 | tf_op jit(solution)/shard_map/ppermute | solution.py:27
  34.5 0.1 collective-permute-start
  34.6 0.5 collective-permute-done.1.refs_5_
  35.1 1.5 %collective-permute-done.2.refs_6_ = bf16[2,8,48,512]{3,2,1,0:T(8,128)(2,1)S(1)} collective-permute-done((bf16[2,8,48,512]{3,2,1,0:T(8,128)(2,1)}, bf16[2,8,48,512]{3,2,1,0:T(8,128)(2,1)S(1)}, u32[]{:S(2)}, u32[]{:S(2)}) %collective-permute-start.2) | collective-permute-done | bytes 786464 | tf_op jit(solution)/shard_map/ppermute | solution.py:27
  36.6 1.1 broadcast_select_fusion.1
  37.6 0.0 collective-permute-start.3
  37.6 0.9 slice.32
  38.5 2.4 %collective-permute-start.4 = (bf16[2,8,32,512]{3,2,1,0:T(8,128)(2,1)}, bf16[2,8,32,512]{3,2,1,0:T(8,128)(2,1)}, u32[]{:S(2)}, u32[]{:S(2)}) collective-permute-start(bf16[2,8,32,512]{3,2,1,0:T(8,128)(2,1)} %slice.32), channel_id=1, source_target_pairs={{0,4},{4,8},{8,12},{12,16},{16,20},{20,24},{24,28},{28,32},{32,36}... | collective-permute-start | bytes 1572872 | tf_op jit(solution)/shard_map/ppermute | solution.py:27
  40.9 0.8 slice.33
  41.8 10.2 %collective-permute-done.11.refs_5_ = bf16[2,8,48,512]{3,2,1,0:T(8,128)(2,1)S(1)} collective-permute-done((bf16[2,8,48,512]{3,2,1,0:T(8,128)(2,1)}, bf16[2,8,48,512]{3,2,1,0:T(8,128)(2,1)S(1)}, u32[]{:S(2)}, u32[]{:S(2)}) %collective-permute-start.11) | collective-permute-done | bytes 786464 | tf_op jit(solution)/shard_map/ppermute | solution.py:27
  51.9 1.9 %collective-permute-start.5 = (bf16[2,8,32,512]{3,2,1,0:T(8,128)(2,1)}, bf16[2,8,32,512]{3,2,1,0:T(8,128)(2,1)}, u32[]{:S(2)}, u32[]{:S(2)}) collective-permute-start(bf16[2,8,32,512]{3,2,1,0:T(8,128)(2,1)} %slice.33), channel_id=1, source_target_pairs={{4,0},{8,4},{12,8},{16,12},{20,16},{24,20},{28,24},{32,28},{36,32}... | collective-permute-start | bytes 1572872 | tf_op jit(solution)/shard_map/ppermute | solution.py:27
  53.8 0.0 collective-permute-done.12.refs_6_
  53.9 0.6 collective-permute-start.10
  54.5 0.1 broadcast_select_fusion
  54.5 0.0 collective-permute-done.refs_3_
  54.6 0.1 collective-permute-start.13
  54.7 0.0 copy-done.2
  54.8 1.7 %collective-permute-done.4.refs_7_ = bf16[2,8,32,512]{3,2,1,0:T(8,128)(2,1)} collective-permute-done((bf16[2,8,32,512]{3,2,1,0:T(8,128)(2,1)}, bf16[2,8,32,512]{3,2,1,0:T(8,128)(2,1)}, u32[]{:S(2)}, u32[]{:S(2)}) %collective-permute-start.4) | collective-permute-done | bytes 524320 | tf_op jit(solution)/shard_map/ppermute | solution.py:27
  56.5 1.9 %collective-permute-start.14 = (bf16[2,8,32,512]{3,2,1,0:T(8,128)(2,1)S(1)}, bf16[2,8,32,512]{3,2,1,0:T(8,128)(2,1)S(1)}, u32[]{:S(2)}, u32[]{:S(2)}) collective-permute-start(bf16[2,8,32,512]{3,2,1,0:T(8,128)(2,1)S(1)} %slice.36), channel_id=1, source_target_pairs={{0,4},{4,8},{8,12},{12,16},{16,20},{20,24},{24,28},{28,32},{32,36}... | collective-permute-start | bytes 1572872 | tf_op jit(solution)/shard_map/ppermute | solution.py:27
  58.4 2.4 %collective-permute-done.5.refs_8_ = bf16[2,8,32,512]{3,2,1,0:T(8,128)(2,1)} collective-permute-done((bf16[2,8,32,512]{3,2,1,0:T(8,128)(2,1)}, bf16[2,8,32,512]{3,2,1,0:T(8,128)(2,1)}, u32[]{:S(2)}, u32[]{:S(2)}) %collective-permute-start.5) | collective-permute-done | bytes 524320 | tf_op jit(solution)/shard_map/ppermute | solution.py:27
  60.8 7.1 %collective-permute-start.15 = (bf16[2,8,32,512]{3,2,1,0:T(8,128)(2,1)S(1)}, bf16[2,8,32,512]{3,2,1,0:T(8,128)(2,1)}, u32[]{:S(2)}, u32[]{:S(2)}) collective-permute-start(bf16[2,8,32,512]{3,2,1,0:T(8,128)(2,1)S(1)} %slice.37), channel_id=1, source_target_pairs={{4,0},{8,4},{12,8},{16,12},{20,16},{24,20},{28,24},{32,28},{36,32}... | collective-permute-start | bytes 1572872 | tf_op jit(solution)/shard_map/ppermute | solution.py:27
  68.0 0.6 pad_add_fusion.refs_0_
  68.6 0.0 collective-permute-done.3.refs_4_
  68.6 7.9 %shard_map.78 = (bf16[2,384,256]{2,1,0:T(8,128)(2,1)}, f32[2,2,384]{2,1,0:T(2,128)}) custom-call(s32[3]{0:T(128)} %pad_add_fusion.refs_0_, bf16[2,8,48,256]{3,2,1,0:T(8,128)(2,1)} %get-tuple-element.10.refs_1_, bf16[2,8,48,512]{3,2,1,0:T(8,128)(2,1)} %get-tuple-element.11.refs_2_, bf16[2,8,48,512]{3,2,1,0:T(8,128)(2,1)} %collective-permute-done.refs_3_, ...), custom_call_target="tpu_custom_call" | custom-call | flops 5284823040 | bytes 4718592 | tf_op jit(solution)/shard_map/pallas_call | solution.py:284
  76.5 1.5 %collective-permute-start.6 = (bf16[2,384,256]{2,1,0:T(8,128)(2,1)}, bf16[2,384,256]{2,1,0:T(8,128)(2,1)S(1)}, u32[]{:S(2)}, u32[]{:S(2)}) collective-permute-start(bf16[2,384,256]{2,1,0:T(8,128)(2,1)} %get-tuple-element.12.refs_1_), channel_id=1, source_target_pairs={{0,1},{1,2},{2,3},{3,0},{4,5},{5,6},{6,7},{7,4},{8,9},{9,10},{10,1... | collective-permute-start | bytes 1179656 | tf_op jit(solution)/shard_map/ppermute | solution.py:32
  78.0 0.0 collective-permute-done.10.refs_3_
  78.0 1.7 %collective-permute-start.7 = (bf16[2,384,256]{2,1,0:T(8,128)(2,1)}, bf16[2,384,256]{2,1,0:T(8,128)(2,1)S(1)}, u32[]{:S(2)}, u32[]{:S(2)}) collective-permute-start(bf16[2,384,256]{2,1,0:T(8,128)(2,1)} %get-tuple-element.12.refs_1_), channel_id=1, source_target_pairs={{0,3},{1,0},{2,1},{3,2},{4,7},{5,4},{6,5},{7,6},{8,11},{9,8},{10,9... | collective-permute-start | bytes 1179656 | tf_op jit(solution)/shard_map/ppermute | solution.py:32
  79.8 0.0 collective-permute-done.14.refs_7_
  79.8 0.0 collective-permute-done.15.refs_8_
  79.8 0.0 collective-permute-done.13.refs_4_
  79.8 0.8 copy-done.15
  80.5 7.9 %shard_map.81 = (bf16[2,384,256]{2,1,0:T(8,128)(2,1)}, f32[2,2,384]{2,1,0:T(2,128)}) custom-call(s32[3]{0:T(128)} %pad_add_fusion.refs_0_, bf16[2,8,48,256]{3,2,1,0:T(8,128)(2,1)} %get-tuple-element.13.refs_1_, bf16[2,8,48,512]{3,2,1,0:T(8,128)(2,1)} %get-tuple-element.14.refs_2_, bf16[2,8,48,512]{3,2,1,0:T(8,128)(2,1)} %collective-permute-done.10.refs_3_, ...), custom_call_target="tpu_custom_call" | custom-call | flops 5284823040 | bytes 4718592 | tf_op jit(solution)/shard_map/pallas_call | solution.py:284
  88.5 0.0 copy-start.14
  88.5 0.4 collective-permute-start.16
  88.8 3.0 %collective-permute-start.17 = (bf16[2,384,256]{2,1,0:T(8,128)(2,1)}, bf16[2,384,256]{2,1,0:T(8,128)(2,1)S(1)}, u32[]{:S(2)}, u32[]{:S(2)}) collective-permute-start(bf16[2,384,256]{2,1,0:T(8,128)(2,1)} %get-tuple-element.15.refs_1_), channel_id=1, source_target_pairs={{0,3},{1,0},{2,1},{3,2},{4,7},{5,4},{6,5},{7,6},{8,11},{9,8},{10,9... | collective-permute-start | bytes 1179656 | tf_op jit(solution)/shard_map/ppermute | solution.py:32
  91.8 0.0 collective-permute-done.6.refs_2_
  91.8 0.1 collective-permute-start.8
  91.9 0.0 collective-permute-done.7.refs_3_
  91.9 3.3 %collective-permute-start.9 = (bf16[2,192,256]{2,1,0:T(8,128)(2,1)S(1)}, bf16[2,192,256]{2,1,0:T(8,128)(2,1)S(1)}, u32[]{:S(2)}, u32[]{:S(2)}) collective-permute-start(bf16[2,192,256]{2,1,0:T(8,128)(2,1)S(1)} %slice.35), channel_id=1, source_target_pairs={{0,3},{1,0},{2,1},{3,2},{4,7},{5,4},{6,5},{7,6},{8,11},{9,8},{10,9... | collective-permute-start | bytes 589832 | tf_op jit(solution)/shard_map/ppermute | solution.py:32
  95.2 4.7 %collective-permute-done.16.refs_2_ = bf16[2,384,256]{2,1,0:T(8,128)(2,1)S(1)} collective-permute-done((bf16[2,384,256]{2,1,0:T(8,128)(2,1)}, bf16[2,384,256]{2,1,0:T(8,128)(2,1)S(1)}, u32[]{:S(2)}, u32[]{:S(2)}) %collective-permute-start.16) | collective-permute-done | bytes 393248 | tf_op jit(solution)/shard_map/ppermute | solution.py:32
  100.0 0.1 collective-permute-start.18
  100.1 0.0 collective-permute-done.17.refs_3_
  100.1 0.0 copy-start.8
  100.1 3.3 %collective-permute-start.19 = (bf16[2,192,256]{2,1,0:T(8,128)(2,1)S(1)}, bf16[2,192,256]{2,1,0:T(8,128)(2,1)S(1)}, u32[]{:S(2)}, u32[]{:S(2)}) collective-permute-start(bf16[2,192,256]{2,1,0:T(8,128)(2,1)S(1)} %slice.39), channel_id=1, source_target_pairs={{0,3},{1,0},{2,1},{3,2},{4,7},{5,4},{6,5},{7,6},{8,11},{9,8},{10,9... | collective-permute-start | bytes 589832 | tf_op jit(solution)/shard_map/ppermute | solution.py:32
  103.4 0.6 pad_maximum_fusion.3
  104.0 0.0 collective-permute-done.8.refs_4_
  104.0 0.0 collective-permute-done.9.refs_5_
  104.1 0.6 copy-done.9
  104.7 0.1 copy-done.11
  104.8 5.1 %shard_map.79 = bf16[2,384,512]{2,1,0:T(8,128)(2,1)} custom-call(s32[3]{0:T(128)} %pad_add_fusion.refs_0_, bf16[2,384,256]{2,1,0:T(8,128)(2,1)} %get-tuple-element.12.refs_1_, bf16[2,384,256]{2,1,0:T(8,128)(2,1)} %copy-done.5, bf16[2,384,256]{2,1,0:T(8,128)(2,1)} %copy-done.6, bf16[2,192,256]{2,1,0:T(8,128)(2,1)} %copy-done.9, ...), custom_call_target="tpu_custom_call" | custom-call | flops 805306368 | bytes 3407872 | tf_op jit(solution)/shard_map/pallas_call | solution.py:362
  109.9 0.0 copy-start
  109.9 0.0 collective-permute-done.18.refs_4_
  109.9 0.0 collective-permute-done.19.refs_5_
  109.9 0.6 copy-done.10
  110.6 0.7 copy-done.12
  111.2 5.1 %shard_map.82 = bf16[2,384,512]{2,1,0:T(8,128)(2,1)} custom-call(s32[3]{0:T(128)} %pad_add_fusion.refs_0_, bf16[2,384,256]{2,1,0:T(8,128)(2,1)} %get-tuple-element.15.refs_1_, bf16[2,384,256]{2,1,0:T(8,128)(2,1)} %copy-done.7, bf16[2,384,256]{2,1,0:T(8,128)(2,1)} %copy-done.8, bf16[2,192,256]{2,1,0:T(8,128)(2,1)} %copy-done.10, ...), custom_call_target="tpu_custom_call" | custom-call | flops 805306368 | bytes 3407872 | tf_op jit(solution)/shard_map/pallas_call | solution.py:362
  116.3 2.4 %pad_maximum_fusion = bf16[4,384,512]{2,1,0:T(8,128)(2,1)} fusion(bf16[2,384,512]{2,1,0:T(8,128)(2,1)} %shard_map.82, bf16[2,384,512]{2,1,0:T(8,128)(2,1)S(1)} %copy-done), kind=kLoop, calls=%fused_computation | loop fusion | flops 786432 | bytes 3145728 | tf_op jit(solution)/shard_map/concatenate | solution.py:423
  (31 shorter events, 0.2 us)
Async XLA Ops:
  9.3 25.8 %collective-permute-start.1 = (bf16[2,8,48,512]{3,2,1,0:T(8,128)(2,1)}, bf16[2,8,48,512]{3,2,1,0:T(8,128)(2,1)S(1)}, u32[]{:S(2)}, u32[]{:S(2)}) collective-permute-start(bf16[2,8,48,512]{3,2,1,0:T(8,128)(2,1)} %get-tuple-element.11.refs_2_), channel_id=1, source_target_pairs={{0,8},{4,12},{8,16},{12,20},{16,24},{20,28},{24,32},{28,36},{32,40... | collective-permute-start | bytes 2359304 | tf_op jit(solution)/shard_map/ppermute | solution.py:27
  12.7 23.8 %collective-permute-start.2 = (bf16[2,8,48,512]{3,2,1,0:T(8,128)(2,1)}, bf16[2,8,48,512]{3,2,1,0:T(8,128)(2,1)S(1)}, u32[]{:S(2)}, u32[]{:S(2)}) collective-permute-start(bf16[2,8,48,512]{3,2,1,0:T(8,128)(2,1)} %get-tuple-element.11.refs_2_), channel_id=1, source_target_pairs={{8,0},{12,4},{16,8},{20,12},{24,16},{28,20},{32,24},{36,28},{40,32... | collective-permute-start | bytes 2359304 | tf_op jit(solution)/shard_map/ppermute | solution.py:27
  25.3 26.6 %collective-permute-start.11 = (bf16[2,8,48,512]{3,2,1,0:T(8,128)(2,1)}, bf16[2,8,48,512]{3,2,1,0:T(8,128)(2,1)S(1)}, u32[]{:S(2)}, u32[]{:S(2)}) collective-permute-start(bf16[2,8,48,512]{3,2,1,0:T(8,128)(2,1)} %get-tuple-element.14.refs_2_), channel_id=1, source_target_pairs={{0,8},{4,12},{8,16},{12,20},{16,24},{20,28},{24,32},{28,36},{32,40... | collective-permute-start | bytes 2359304 | tf_op jit(solution)/shard_map/ppermute | solution.py:27
  27.3 26.6 %collective-permute-start.12 = (bf16[2,8,48,512]{3,2,1,0:T(8,128)(2,1)}, bf16[2,8,48,512]{3,2,1,0:T(8,128)(2,1)S(1)}, u32[]{:S(2)}, u32[]{:S(2)}) collective-permute-start(bf16[2,8,48,512]{3,2,1,0:T(8,128)(2,1)} %get-tuple-element.14.refs_2_), channel_id=1, source_target_pairs={{8,0},{12,4},{16,8},{20,12},{24,16},{28,20},{32,24},{36,28},{40,32... | collective-permute-start | bytes 2359304 | tf_op jit(solution)/shard_map/ppermute | solution.py:27
  34.5 20.0 %collective-permute-start = (bf16[2,8,48,512]{3,2,1,0:T(8,128)(2,1)}, bf16[2,8,48,512]{3,2,1,0:T(8,128)(2,1)}, u32[]{:S(2)}, u32[]{:S(2)}) collective-permute-start(bf16[2,8,48,512]{3,2,1,0:T(8,128)(2,1)} %get-tuple-element.11.refs_2_), channel_id=1, source_target_pairs={{0,4},{4,0},{8,12},{12,8},{16,20},{20,16},{24,28},{28,24},{32,36},... | collective-permute-start | bytes 2359304 | tf_op jit(solution)/shard_map/ppermute | solution.py:36
  35.1 3.4 %copy-start.3 = (bf16[2,8,48,512]{3,2,1,0:T(8,128)(2,1)}, bf16[2,8,48,512]{3,2,1,0:T(8,128)(2,1)S(1)}, u32[]{:S(2)}) copy-start(bf16[2,8,48,512]{3,2,1,0:T(8,128)(2,1)S(1)} %collective-permute-done.1.refs_5_) | copy-start | bytes 2359300
  36.5 4.4 %copy-start.4 = (bf16[2,8,48,512]{3,2,1,0:T(8,128)(2,1)}, bf16[2,8,48,512]{3,2,1,0:T(8,128)(2,1)S(1)}, u32[]{:S(2)}) copy-start(bf16[2,8,48,512]{3,2,1,0:T(8,128)(2,1)S(1)} %collective-permute-done.2.refs_6_) | copy-start | bytes 2359300
  37.6 31.0 %collective-permute-start.3 = (bf16[2,8,48,512]{3,2,1,0:T(8,128)(2,1)}, bf16[2,8,48,512]{3,2,1,0:T(8,128)(2,1)}, u32[]{:S(2)}, u32[]{:S(2)}) collective-permute-start(bf16[2,8,48,512]{3,2,1,0:T(8,128)(2,1)} %broadcast_select_fusion.1), channel_id=1, source_target_pairs={{0,4},{4,0},{8,12},{12,8},{16,20},{20,16},{24,28},{28,24},{32,36},... | collective-permute-start | bytes 2359304 | tf_op jit(solution)/shard_map/ppermute | solution.py:36
  38.5 18.0 %collective-permute-start.4 = (bf16[2,8,32,512]{3,2,1,0:T(8,128)(2,1)}, bf16[2,8,32,512]{3,2,1,0:T(8,128)(2,1)}, u32[]{:S(2)}, u32[]{:S(2)}) collective-permute-start(bf16[2,8,32,512]{3,2,1,0:T(8,128)(2,1)} %slice.32), channel_id=1, source_target_pairs={{0,4},{4,8},{8,12},{12,16},{16,20},{20,24},{24,28},{28,32},{32,36}... | collective-permute-start | bytes 1572872 | tf_op jit(solution)/shard_map/ppermute | solution.py:27
  51.9 2.8 %copy-start.1 = (bf16[2,8,48,512]{3,2,1,0:T(8,128)(2,1)}, bf16[2,8,48,512]{3,2,1,0:T(8,128)(2,1)S(1)}, u32[]{:S(2)}) copy-start(bf16[2,8,48,512]{3,2,1,0:T(8,128)(2,1)S(1)} %collective-permute-done.11.refs_5_) | copy-start | bytes 2359300
  51.9 8.9 %collective-permute-start.5 = (bf16[2,8,32,512]{3,2,1,0:T(8,128)(2,1)}, bf16[2,8,32,512]{3,2,1,0:T(8,128)(2,1)}, u32[]{:S(2)}, u32[]{:S(2)}) collective-permute-start(bf16[2,8,32,512]{3,2,1,0:T(8,128)(2,1)} %slice.33), channel_id=1, source_target_pairs={{4,0},{8,4},{12,8},{16,12},{20,16},{24,20},{28,24},{32,28},{36,32}... | collective-permute-start | bytes 1572872 | tf_op jit(solution)/shard_map/ppermute | solution.py:27
  53.9 0.9 copy-start.2
  53.9 24.2 %collective-permute-start.10 = (bf16[2,8,48,512]{3,2,1,0:T(8,128)(2,1)}, bf16[2,8,48,512]{3,2,1,0:T(8,128)(2,1)}, u32[]{:S(2)}, u32[]{:S(2)}) collective-permute-start(bf16[2,8,48,512]{3,2,1,0:T(8,128)(2,1)} %get-tuple-element.14.refs_2_), channel_id=1, source_target_pairs={{0,4},{4,0},{8,12},{12,8},{16,20},{20,16},{24,28},{28,24},{32,36},... | collective-permute-start | bytes 2359304 | tf_op jit(solution)/shard_map/ppermute | solution.py:36
  54.6 25.2 %collective-permute-start.13 = (bf16[2,8,48,512]{3,2,1,0:T(8,128)(2,1)S(1)}, bf16[2,8,48,512]{3,2,1,0:T(8,128)(2,1)}, u32[]{:S(2)}, u32[]{:S(2)}) collective-permute-start(bf16[2,8,48,512]{3,2,1,0:T(8,128)(2,1)S(1)} %broadcast_select_fusion), channel_id=1, source_target_pairs={{0,4},{4,0},{8,12},{12,8},{16,20},{20,16},{24,28},{28,24},{32,36},... | collective-permute-start | bytes 2359304 | tf_op jit(solution)/shard_map/ppermute | solution.py:36
  56.5 23.2 %collective-permute-start.14 = (bf16[2,8,32,512]{3,2,1,0:T(8,128)(2,1)S(1)}, bf16[2,8,32,512]{3,2,1,0:T(8,128)(2,1)S(1)}, u32[]{:S(2)}, u32[]{:S(2)}) collective-permute-start(bf16[2,8,32,512]{3,2,1,0:T(8,128)(2,1)S(1)} %slice.36), channel_id=1, source_target_pairs={{0,4},{4,8},{8,12},{12,16},{16,20},{20,24},{24,28},{28,32},{32,36}... | collective-permute-start | bytes 1572872 | tf_op jit(solution)/shard_map/ppermute | solution.py:27
  60.8 18.9 %collective-permute-start.15 = (bf16[2,8,32,512]{3,2,1,0:T(8,128)(2,1)S(1)}, bf16[2,8,32,512]{3,2,1,0:T(8,128)(2,1)}, u32[]{:S(2)}, u32[]{:S(2)}) collective-permute-start(bf16[2,8,32,512]{3,2,1,0:T(8,128)(2,1)S(1)} %slice.37), channel_id=1, source_target_pairs={{4,0},{8,4},{12,8},{16,12},{20,16},{24,20},{28,24},{32,28},{36,32}... | collective-permute-start | bytes 1572872 | tf_op jit(solution)/shard_map/ppermute | solution.py:27
  76.5 15.3 %collective-permute-start.6 = (bf16[2,384,256]{2,1,0:T(8,128)(2,1)}, bf16[2,384,256]{2,1,0:T(8,128)(2,1)S(1)}, u32[]{:S(2)}, u32[]{:S(2)}) collective-permute-start(bf16[2,384,256]{2,1,0:T(8,128)(2,1)} %get-tuple-element.12.refs_1_), channel_id=1, source_target_pairs={{0,1},{1,2},{2,3},{3,0},{4,5},{5,6},{6,7},{7,4},{8,9},{9,10},{10,1... | collective-permute-start | bytes 1179656 | tf_op jit(solution)/shard_map/ppermute | solution.py:32
  78.0 13.9 %collective-permute-start.7 = (bf16[2,384,256]{2,1,0:T(8,128)(2,1)}, bf16[2,384,256]{2,1,0:T(8,128)(2,1)S(1)}, u32[]{:S(2)}, u32[]{:S(2)}) collective-permute-start(bf16[2,384,256]{2,1,0:T(8,128)(2,1)} %get-tuple-element.12.refs_1_), channel_id=1, source_target_pairs={{0,3},{1,0},{2,1},{3,2},{4,7},{5,4},{6,5},{7,6},{8,11},{9,8},{10,9... | collective-permute-start | bytes 1179656 | tf_op jit(solution)/shard_map/ppermute | solution.py:32
  79.8 0.8 copy-start.15
  88.5 15.0 %copy-start.13 = (f32[2,2,384]{2,1,0:T(2,128)S(1)}, f32[2,2,384]{2,1,0:T(2,128)}, u32[]{:S(2)}) copy-start(f32[2,2,384]{2,1,0:T(2,128)} %get-tuple-element.16) | copy-start | bytes 18436
  88.5 15.0 %copy-start.14 = (f32[2,2,384]{2,1,0:T(2,128)S(1)}, f32[2,2,384]{2,1,0:T(2,128)}, u32[]{:S(2)}) copy-start(f32[2,2,384]{2,1,0:T(2,128)} %get-tuple-element.17) | copy-start | bytes 18436
  88.5 11.5 %collective-permute-start.16 = (bf16[2,384,256]{2,1,0:T(8,128)(2,1)}, bf16[2,384,256]{2,1,0:T(8,128)(2,1)S(1)}, u32[]{:S(2)}, u32[]{:S(2)}) collective-permute-start(bf16[2,384,256]{2,1,0:T(8,128)(2,1)} %get-tuple-element.15.refs_1_), channel_id=1, source_target_pairs={{0,1},{1,2},{2,3},{3,0},{4,5},{5,6},{6,7},{7,4},{8,9},{9,10},{10,1... | collective-permute-start | bytes 1179656 | tf_op jit(solution)/shard_map/ppermute | solution.py:32
  88.8 11.3 %collective-permute-start.17 = (bf16[2,384,256]{2,1,0:T(8,128)(2,1)}, bf16[2,384,256]{2,1,0:T(8,128)(2,1)S(1)}, u32[]{:S(2)}, u32[]{:S(2)}) collective-permute-start(bf16[2,384,256]{2,1,0:T(8,128)(2,1)} %get-tuple-element.15.refs_1_), channel_id=1, source_target_pairs={{0,3},{1,0},{2,1},{3,2},{4,7},{5,4},{6,5},{7,6},{8,11},{9,8},{10,9... | collective-permute-start | bytes 1179656 | tf_op jit(solution)/shard_map/ppermute | solution.py:32
  91.8 12.3 %copy-start.5 = (bf16[2,384,256]{2,1,0:T(8,128)(2,1)}, bf16[2,384,256]{2,1,0:T(8,128)(2,1)S(1)}, u32[]{:S(2)}) copy-start(bf16[2,384,256]{2,1,0:T(8,128)(2,1)S(1)} %collective-permute-done.6.refs_2_) | copy-start | bytes 1179652
  91.8 12.2 %collective-permute-start.8 = (bf16[2,192,256]{2,1,0:T(8,128)(2,1)S(1)}, bf16[2,192,256]{2,1,0:T(8,128)(2,1)S(1)}, u32[]{:S(2)}, u32[]{:S(2)}) collective-permute-start(bf16[2,192,256]{2,1,0:T(8,128)(2,1)S(1)} %slice.34), channel_id=1, source_target_pairs={{0,1},{1,2},{2,3},{3,0},{4,5},{5,6},{6,7},{7,4},{8,9},{9,10},{10,1... | collective-permute-start | bytes 589832 | tf_op jit(solution)/shard_map/ppermute | solution.py:32
  91.9 12.1 %copy-start.6 = (bf16[2,384,256]{2,1,0:T(8,128)(2,1)}, bf16[2,384,256]{2,1,0:T(8,128)(2,1)S(1)}, u32[]{:S(2)}) copy-start(bf16[2,384,256]{2,1,0:T(8,128)(2,1)S(1)} %collective-permute-done.7.refs_3_) | copy-start | bytes 1179652
  91.9 12.1 %collective-permute-start.9 = (bf16[2,192,256]{2,1,0:T(8,128)(2,1)S(1)}, bf16[2,192,256]{2,1,0:T(8,128)(2,1)S(1)}, u32[]{:S(2)}, u32[]{:S(2)}) collective-permute-start(bf16[2,192,256]{2,1,0:T(8,128)(2,1)S(1)} %slice.35), channel_id=1, source_target_pairs={{0,3},{1,0},{2,1},{3,2},{4,7},{5,4},{6,5},{7,6},{8,11},{9,8},{10,9... | collective-permute-start | bytes 589832 | tf_op jit(solution)/shard_map/ppermute | solution.py:32
  100.0 9.9 %copy-start.7 = (bf16[2,384,256]{2,1,0:T(8,128)(2,1)}, bf16[2,384,256]{2,1,0:T(8,128)(2,1)S(1)}, u32[]{:S(2)}) copy-start(bf16[2,384,256]{2,1,0:T(8,128)(2,1)S(1)} %collective-permute-done.16.refs_2_) | copy-start | bytes 1179652
  100.0 9.9 %collective-permute-start.18 = (bf16[2,192,256]{2,1,0:T(8,128)(2,1)S(1)}, bf16[2,192,256]{2,1,0:T(8,128)(2,1)S(1)}, u32[]{:S(2)}, u32[]{:S(2)}) collective-permute-start(bf16[2,192,256]{2,1,0:T(8,128)(2,1)S(1)} %slice.38), channel_id=1, source_target_pairs={{0,1},{1,2},{2,3},{3,0},{4,5},{5,6},{6,7},{7,4},{8,9},{9,10},{10,1... | collective-permute-start | bytes 589832 | tf_op jit(solution)/shard_map/ppermute | solution.py:32
  100.1 9.8 %copy-start.8 = (bf16[2,384,256]{2,1,0:T(8,128)(2,1)}, bf16[2,384,256]{2,1,0:T(8,128)(2,1)S(1)}, u32[]{:S(2)}) copy-start(bf16[2,384,256]{2,1,0:T(8,128)(2,1)S(1)} %collective-permute-done.17.refs_3_) | copy-start | bytes 1179652
  100.1 9.8 %collective-permute-start.19 = (bf16[2,192,256]{2,1,0:T(8,128)(2,1)S(1)}, bf16[2,192,256]{2,1,0:T(8,128)(2,1)S(1)}, u32[]{:S(2)}, u32[]{:S(2)}) collective-permute-start(bf16[2,192,256]{2,1,0:T(8,128)(2,1)S(1)} %slice.39), channel_id=1, source_target_pairs={{0,3},{1,0},{2,1},{3,2},{4,7},{5,4},{6,5},{7,6},{8,11},{9,8},{10,9... | collective-permute-start | bytes 589832 | tf_op jit(solution)/shard_map/ppermute | solution.py:32
  104.0 0.7 copy-start.9
  104.0 0.7 copy-start.11
  109.9 6.5 %copy-start = (bf16[2,384,512]{2,1,0:T(8,128)(2,1)S(1)}, bf16[2,384,512]{2,1,0:T(8,128)(2,1)}, u32[]{:S(2)}) copy-start(bf16[2,384,512]{2,1,0:T(8,128)(2,1)} %shard_map.79) | copy-start | bytes 2359300
  109.9 0.7 copy-start.10
  110.6 0.7 copy-start.12
